TPU v7x, 32 devices: a whole 2x2x4 slice. The times are simulated.
32 devices in a mesh: ep: 4 (over y, x), tp: 8 (over z, core).
Axes of the slice: x: 2, y: 2, z: 4, core: 2. Of those that a mesh axis runs over, the one named last changes fastest.
Arguments:
- tokens: bfloat16 [4096, 2048], P('ep', 'tp'), may hold values from -48 to 48
- pre_gain: bfloat16 [2048], P('tp'), may hold values from 0.099609375 to 1.8984375
- route_ids: int32 [4096, 2], P('ep'), may hold values from 0 to 3, all different within a row; in each aligned block of 1024 rows (0 to 1023, 1024 to 2047, ...) at most 576 rows name the same one
- route_weights: float32 [4096, 2], P('ep'), may hold values from 0.1 to 1
- gate_weight: bfloat16 [4, 2048, 7168], P('ep', None, 'tp'), may hold values from -0.125 to 0.125
- up_weight: bfloat16 [4, 2048, 7168], P('ep', None, 'tp'), may hold values from -0.125 to 0.125
- down_weight: bfloat16 [4, 7168, 2048], P('ep', 'tp')
- post_gain: bfloat16 [2048], P('tp'), may hold values from 0.099609375 to 1.8984375
Outputs:
- mixed: bfloat16 [4096, 2048], P('ep', 'tp')
Inputs may be any that keep to these rules, and one draw needn't show every extreme that they name: `route_ids`: each row names 2 different experts; among the rows of one index of ep no expert is named more than 576 times, a bound that some block reaches.
All inputs are finite; a program needn't handle non-finite values.
Results may differ from a plain program's by a relative error of at most 0.02.
Values may be sent and summed in bfloat16 or wider, within the bound.
A program may use at most 128 MiB of HBM per device.

v0:
```python
import functools

import jax
import jax.numpy as jnp
from jax import lax
from jax.experimental import pallas as pl
from jax.experimental.pallas import tpu as pltpu
from jax.sharding import PartitionSpec as P

epsilon = 1e-06
MESH = pl.DeviceIdType.MESH
DMA = pltpu.SemaphoreType.DMA
BF16 = jnp.bfloat16


def greet(targets):
    barrier = pltpu.get_barrier_semaphore()
    for target in targets:
        pl.semaphore_signal(barrier, inc=1, device_id=target, device_id_type=MESH)
    pl.semaphore_wait(barrier, len(targets))


def exchange_kernel(n, x_ref, out_ref, buf, send, recv):
    me = lax.axis_index("tp")
    peers = [{"tp": lax.rem(me + k, n)} for k in range(1, n)]
    greet(peers)
    copies = []
    for k in range(1, n):
        copy = pltpu.make_async_remote_copy(
            src_ref=x_ref, dst_ref=buf.at[k - 1], send_sem=send.at[k - 1],
            recv_sem=recv.at[k - 1], device_id=peers[k - 1], device_id_type=MESH,
        )
        copy.start()
        copies.append(copy)
    total = x_ref[...]
    for k in range(1, n):
        copies[k - 1].wait_recv()
        total = total + buf[k - 1]
    out_ref[...] = total
    for copy in copies:
        copy.wait_send()


def sum_over_tp(rows, number):
    n = lax.axis_size("tp")
    x = rows.reshape(-1, 128)
    total = pl.pallas_call(
        functools.partial(exchange_kernel, n),
        out_shape=jax.ShapeDtypeStruct(x.shape, jnp.float32),
        in_specs=[pl.BlockSpec(memory_space=pltpu.VMEM)],
        out_specs=pl.BlockSpec(memory_space=pltpu.VMEM),
        scratch_shapes=[pltpu.VMEM((n - 1,) + x.shape, jnp.float32), DMA((n - 1,)), DMA((n - 1,))],
        compiler_params=pltpu.CompilerParams(collective_id=number, has_side_effects=True),
        name="exchange%d" % number,
    )(x)
    return total.reshape(-1)


def places(groups, layers):
    me, g = lax.axis_index("tp"), lax.axis_index("ep")
    core, z = lax.rem(me, 2), me // 2
    return core, z, g, {"tp": me + 1 - 2 * core}


def greet_all(groups, layers, core, z, g, partner):
    targets = [partner]
    targets += [{"tp": lax.rem(z + k, layers) * 2 + core} for k in range(1, layers)]
    targets += [{"ep": lax.rem(g + m, groups)} for m in range(1, groups)]
    greet(targets)


def dispatch_kernel(
    groups, layers, cap, cols, tile, x_ref, key_ref, gate_ref, up_ref, out_ref,
    zbuf, obuf, sbuf, piece, wbuf, acc, zs, zr, es, er, ds, dr, ws,
):
    core, z, g, partner = places(groups, layers)
    loads = [
        pltpu.make_async_copy(ref, wbuf.at[i], ws.at[i]) for i, ref in enumerate((gate_ref, up_ref))
    ]
    for load in loads:
        load.start()
    greet_all(groups, layers, core, z, g, partner)

    def z_copy(source, to, at, sem):
        return pltpu.make_async_remote_copy(
            src_ref=source, dst_ref=zbuf.at[at], send_sem=zs.at[sem], recv_sem=zr.at[at],
            device_id={"tp": to * 2 + core}, device_id_type=MESH,
        )

    def slot(s):
        inner = jnp.minimum(z, layers - 1 - z)
        near = jnp.where(s % 2 == 1, (s + 1) // 2, layers - (s + 1) // 2)
        far = jnp.where(2 * z > layers - 1, s - inner, layers - s + inner)
        return jnp.where(s == 0, 0, jnp.where(s <= 2 * inner, near, far))

    to_right = z_copy(x_ref, z + 1, 1, 0)
    to_left = z_copy(x_ref, z - 1, layers - 1, layers)

    def relays(k):
        right = jnp.logical_and(jnp.logical_and(k > 0, z >= k), z < layers - 1)
        left = jnp.logical_and(z < k, z > 0)
        return (
            (right, z_copy(zbuf.at[k], z + 1, k + 1, k)),
            (left, z_copy(zbuf.at[k], z - 1, k - 1, k)),
        )

    def area(k, m):
        source = lax.rem(g + groups - m, groups)
        return piece.at[core, k, pl.ds(pl.multiple_of(source * cap, 16), cap)]

    def e_copy(k, m):
        return pltpu.make_async_remote_copy(
            src_ref=obuf.at[k, m], dst_ref=area(k, 0), send_sem=es.at[k, m],
            recv_sem=er.at[k, m], device_id={"ep": lax.rem(g + m, groups)}, device_id_type=MESH,
        )

    def d_copy(k, m):
        return pltpu.make_async_remote_copy(
            src_ref=area(k, m), dst_ref=area(k, m), send_sem=ds.at[k, m],
            recv_sem=dr.at[k, m], device_id=partner, device_id_type=MESH,
        )

    pl.when(z < layers - 1)(to_right.start)
    pl.when(z > 0)(to_left.start)
    zbuf[0] = x_ref[...]

    def build(e):
        wanted = lax.broadcasted_iota(jnp.int32, (cap, key_ref.shape[2]), 0)
        sbuf[e] = jnp.where(key_ref[e] == wanted, 1.0, 0.0).astype(BF16)

    def finish(s):
        k = slot(s)

        @pl.loop(1, groups)
        def _(m):
            e_copy(k, m).wait_recv()
            d_copy(k, m).start()

        @pl.loop(0, groups)
        def _(m):
            d_copy(k, m).wait_recv()

        block = lax.rem(z + layers - k, layers)
        depth = pl.ds(pl.multiple_of(block * 2 * cols, 128), 2 * cols)

        @pl.loop(0, groups * cap // tile)
        def _(t):
            at = pl.ds(pl.multiple_of(t * tile, tile), tile)
            left = jnp.concatenate([piece[0, k, at], piece[1, k, at]], axis=1)
            gate = jnp.dot(left, wbuf[0, depth], preferred_element_type=jnp.float32)
            up = jnp.dot(left, wbuf[1, depth], preferred_element_type=jnp.float32)

            @pl.when(s == 0)
            def _():
                acc[0, at] = gate
                acc[1, at] = up

            @pl.when(jnp.logical_and(s > 0, s < layers - 1))
            def _():
                acc[0, at] += gate
                acc[1, at] += up

            @pl.when(s == layers - 1)
            def _():
                gates = acc[0, at] + gate
                out_ref[at] = (gates / (1.0 + jnp.exp(-gates)) * (acc[1, at] + up)).astype(BF16)

    @pl.loop(0, layers)
    def _(s):
        k = slot(s)

        @pl.when(s > 0)
        def _():
            z_copy(x_ref, lax.rem(z + 1, layers), k, k).wait_recv()
            for wanted, copy in relays(k):
                pl.when(wanted)(copy.start)

        @pl.loop(0, groups)
        def _(i):
            m = lax.rem(i + 1, groups)
            e = lax.rem(g + m, groups)

            @pl.when(s == 0)
            def _():
                build(e)

            tile_out = jnp.dot(sbuf[e], zbuf[k], preferred_element_type=jnp.float32).astype(BF16)

            @pl.when(m > 0)
            def _():
                obuf[k, m] = tile_out
                e_copy(k, m).start()

            @pl.when(m == 0)
            def _():
                piece[core, k, pl.ds(pl.multiple_of(g * cap, 16), cap)] = tile_out

        d_copy(k, 0).start()

        @pl.when(s == 1)
        def _():
            for load in loads:
                load.wait()

        @pl.when(s > 0)
        def _():
            finish(s - 1)

    finish(layers - 1)
    pl.when(z < layers - 1)(to_right.wait_send)
    pl.when(z > 0)(to_left.wait_send)

    @pl.loop(0, layers)
    def _(k):
        for wanted, copy in relays(k):
            pl.when(wanted)(copy.wait_send)

        @pl.loop(0, groups)
        def _(m):
            @pl.when(m > 0)
            def _():
                e_copy(k, m).wait_send()

            d_copy(k, m).wait_send()


def tile_of(rows, cap):
    return 384 if rows % 384 == 0 else cap


def dispatch(normed, key, cap, gate_weight, up_weight):
    tok_rows, groups = key.shape
    layers = lax.axis_size("tp") // 2
    cols = normed.shape[1]
    rows = groups * cap
    units = gate_weight.shape[1]
    vmem = pl.BlockSpec(memory_space=pltpu.VMEM)
    hbm = pl.BlockSpec(memory_space=pl.ANY)
    return pl.pallas_call(
        functools.partial(dispatch_kernel, groups, layers, cap, cols, tile_of(rows, cap)),
        out_shape=jax.ShapeDtypeStruct((rows, units), BF16),
        in_specs=[vmem, vmem, hbm, hbm],
        out_specs=vmem,
        scratch_shapes=[
            pltpu.VMEM((layers, tok_rows, cols), BF16),
            pltpu.VMEM((layers, groups, cap, cols), BF16),
            pltpu.VMEM((groups, cap, tok_rows), BF16),
            pltpu.VMEM((2, layers, rows, cols), BF16),
            pltpu.VMEM((2,) + gate_weight.shape, BF16),
            pltpu.VMEM((2, rows, units), jnp.float32),
            DMA((layers + 1,)), DMA((layers,)),
            DMA((layers, groups)), DMA((layers, groups)),
            DMA((layers, groups)), DMA((layers, groups)),
            DMA((2,)),
        ],
        compiler_params=pltpu.CompilerParams(
            collective_id=1, has_side_effects=True, vmem_limit_bytes=60 * 2**20
        ),
        name="dispatch",
    )(normed, key.T.reshape(groups, 1, tok_rows), gate_weight, up_weight)


def return_kernel(
    groups, layers, cap, cols, tile, h_ref, down_ref, key_ref, weight_ref, out_ref,
    wbuf, mix, lbuf, sbuf, pbuf, qbuf, rbuf, obuf, fbuf, ws, ds, dr, es, er, zs, zr,
):
    core, z, g, partner = places(groups, layers)
    rows = groups * cap

    def w_copy(k, other):
        of = 1 - core if other else core
        column = (lax.rem(z + k, layers) * 2 + of) * cols
        return pltpu.make_async_copy(
            down_ref.at[:, pl.ds(pl.multiple_of(column, 128), cols)], wbuf.at[k, other], ws.at[k, other]
        )

    @pl.loop(0, layers)
    def _(i):
        k = lax.rem(i + 1, layers)
        w_copy(k, 1).start()
        w_copy(k, 0).start()

    greet_all(groups, layers, core, z, g, partner)

    def d_copy(k):
        return pltpu.make_async_remote_copy(
            src_ref=sbuf.at[k], dst_ref=pbuf.at[k], send_sem=ds.at[k],
            recv_sem=dr.at[k], device_id=partner, device_id_type=MESH,
        )

    def e_copy(k, m):
        return pltpu.make_async_remote_copy(
            src_ref=qbuf.at[k, m], dst_ref=rbuf.at[k, pl.ds(pl.multiple_of(g * cap, 16), cap)],
            send_sem=es.at[k, m], recv_sem=er.at[k, m],
            device_id={"ep": lax.rem(g + m, groups)}, device_id_type=MESH,
        )

    def z_copy(k):
        return pltpu.make_async_remote_copy(
            src_ref=obuf.at[k], dst_ref=fbuf.at[k], send_sem=zs.at[k], recv_sem=zr.at[k],
            device_id={"tp": lax.rem(z + k, layers) * 2 + core}, device_id_type=MESH,
        )

    def project(k, other, target):
        @pl.loop(0, rows // tile)
        def _(t):
            at = pl.ds(pl.multiple_of(t * tile, tile), tile)
            target[k, at] = jnp.dot(
                h_ref[at], wbuf[k, other], preferred_element_type=jnp.float32
            ).astype(BF16)

    @pl.loop(0, layers)
    def _(i):
        k = lax.rem(i + 1, layers)
        w_copy(k, 1).wait()
        project(k, 1, sbuf)
        d_copy(k).start()
        w_copy(k, 0).wait()
        project(k, 0, lbuf)
        d_copy(k).wait_recv()

        @pl.loop(0, groups)
        def _(j):
            m = lax.rem(j + 1, groups)
            at = pl.ds(pl.multiple_of(lax.rem(g + m, groups) * cap, 16), cap)
            both = lbuf[k, at].astype(jnp.float32) + pbuf[k, at].astype(jnp.float32)

            @pl.when(m > 0)
            def _():
                qbuf[k, m] = both.astype(BF16)
                e_copy(k, m).start()

            @pl.when(m == 0)
            def _():
                rbuf[k, pl.ds(pl.multiple_of(g * cap, 16), cap)] = both.astype(BF16)

        @pl.when(i == 0)
        def _():
            slots = lax.broadcasted_iota(jnp.int32, (mix.shape[1], cap), 1)
            for e in range(groups):
                mix[e] = jnp.where(
                    key_ref[:, e : e + 1] == slots, weight_ref[:, e : e + 1], 0.0
                ).astype(BF16)

    tok_rows = mix.shape[1]
    step = min(256, tok_rows)

    @pl.loop(0, layers)
    def _(i):
        k = lax.rem(i + 1, layers)

        @pl.loop(1, groups)
        def _(m):
            e_copy(k, m).wait_recv()

        @pl.loop(0, tok_rows // step)
        def _(t):
            at = pl.ds(pl.multiple_of(t * step, step), step)
            value = jnp.zeros((step, cols), jnp.float32)
            for e in range(groups):
                value += jnp.dot(
                    mix[e, at], rbuf[k, e * cap : (e + 1) * cap], preferred_element_type=jnp.float32
                )

            @pl.when(k > 0)
            def _():
                obuf[k, at] = value.astype(BF16)

            @pl.when(k == 0)
            def _():
                out_ref[at] = value

        @pl.when(k > 0)
        def _():
            z_copy(k).start()

    @pl.loop(1, layers)
    def _(k):
        z_copy(k).wait_recv()
        out_ref[...] += fbuf[k].astype(jnp.float32)

    @pl.loop(0, layers)
    def _(k):
        d_copy(k).wait_send()

        @pl.loop(1, groups)
        def _(m):
            e_copy(k, m).wait_send()

        @pl.when(k > 0)
        def _():
            z_copy(k).wait_send()


def give_back(hidden, down_weight, key, weight):
    rows, units = hidden.shape
    tok_rows, groups = key.shape
    layers = lax.axis_size("tp") // 2
    cols = down_weight.shape[1] // (2 * layers)
    cap = rows // groups
    vmem = pl.BlockSpec(memory_space=pltpu.VMEM)
    hbm = pl.BlockSpec(memory_space=pl.ANY)
    whole = pltpu.VMEM((layers, rows, cols), BF16)
    return pl.pallas_call(
        functools.partial(return_kernel, groups, layers, cap, cols, tile_of(rows, cap)),
        out_shape=jax.ShapeDtypeStruct((tok_rows, cols), jnp.float32),
        in_specs=[vmem, hbm, vmem, vmem],
        out_specs=vmem,
        scratch_shapes=[
            pltpu.VMEM((layers, 2, units, cols), BF16),
            pltpu.VMEM((groups, tok_rows, cap), BF16),
            whole, whole, whole,
            pltpu.VMEM((layers, groups, cap, cols), BF16),
            whole,
            pltpu.VMEM((layers, tok_rows, cols), BF16),
            pltpu.VMEM((layers, tok_rows, cols), BF16),
            DMA((layers, 2)), DMA((layers,)), DMA((layers,)),
            DMA((layers, groups)), DMA((layers, groups)),
            DMA((layers,)), DMA((layers,)),
        ],
        compiler_params=pltpu.CompilerParams(
            collective_id=2, has_side_effects=True, vmem_limit_bytes=60 * 2**20
        ),
        name="give_back",
    )(hidden, down_weight, key, weight)


def on_device(
    tokens, pre_gain, route_ids, route_weights, gate_weight, up_weight, down_weight, post_gain
):
    tok_rows, cols = tokens.shape
    top_count = route_ids.shape[1]
    groups = lax.axis_size("ep")
    width = cols * lax.axis_size("tp")
    cap = 9 * tok_rows * top_count // (8 * groups)
    values = tokens.astype(jnp.float32)
    squares = sum_over_tp(jnp.sum(values * values, axis=1), 0)
    normed = (
        values * lax.rsqrt(squares / width + epsilon)[:, None] * pre_gain.astype(jnp.float32)[None, :]
    ).astype(BF16)

    experts = jnp.arange(groups, dtype=jnp.int32)
    named = route_ids[:, :, None] == experts[None, None, :]
    member = jnp.any(named, axis=1)
    weight = jnp.sum(jnp.where(named, route_weights[:, :, None], 0.0), axis=1)
    spot = jnp.arange(tok_rows, dtype=jnp.int32)
    before = (spot[:, None] > spot[None, :]).astype(BF16)
    rank = jnp.dot(before, member.astype(BF16), preferred_element_type=jnp.float32)
    key = jnp.where(member, rank.astype(jnp.int32), -1)

    hidden = dispatch(normed, key, cap, gate_weight[0], up_weight[0])
    combined = give_back(hidden, down_weight[0], key, weight)
    totals = sum_over_tp(jnp.sum(combined * combined, axis=1), 3)
    scaled = combined * lax.rsqrt(totals / width + epsilon)[:, None]
    return (scaled * post_gain.astype(jnp.float32)[None, :]).astype(BF16)


def solution(mesh):
    placed = (
        P("ep", "tp"),
        P("tp"),
        P("ep", None),
        P("ep", None),
        P("ep", None, "tp"),
        P("ep", None, "tp"),
        P("ep", "tp", None),
        P("tp"),
    )
    return jax.shard_map(
        on_device, mesh=mesh, in_specs=placed, out_specs=P("ep", "tp"), check_vma=False
    )
```

profile of v0, /device:TPU:0, one launch (start us, length us, event | category | flops | bytes accessed | tf_op | source)
XLA Modules:
  0.0 190.1 jit_solution(12789815820155615545)
XLA Ops:
  0.0 0.7 fusion.6
  0.7 0.3 copy.14
  1.0 0.7 fusion.2.key_ref
  1.7 0.0 copy-start
  1.7 0.8 copy.15.key_ref
  2.5 1.8 fusion.3
  4.4 8.7 %exchange0.1 = f32[8,128]{1,0:T(8,128)} custom-call(f32[8,128]{1,0:T(8,128)} %bitcast.17), custom_call_target="tpu_custom_call" | custom-call | tf_op jit(solution)/shard_map/exchange0/pallas_call | solution.py:47
  13.1 0.7 rsqrt_bitcast_fusion.1
  13.7 0.7 convert_element_type.23
  14.4 2.0 %fusion.5.x_ref = bf16[1024,256]{1,0:T(8,128)(2,1)} fusion(bf16[1024,256]{1,0:T(8,128)(2,1)} %param.8, f32[256]{0:T(256)S(1)} %convert_element_type.23, f32[1024]{0:T(1024)S(1)} %rsqrt_bitcast_fusion.1), kind=kLoop, calls=%fused_computation.8 | loop fusion | flops 1048576 | bytes 1053696 | tf_op jit(solution)/shard_map/convert_element_type | solution.py:440
  16.4 0.0 copy-start.1
  16.5 0.0 copy-start.2
  16.5 81.4 %dispatch.1.h_ref = bf16[2304,896]{1,0:T(8,128)(2,1)} custom-call(bf16[1024,256]{1,0:T(8,128)(2,1)} %fusion.5.x_ref, s32[4,1,1024]{2,1,0:T(1,128)} %copy.15.key_ref, bf16[2048,896]{1,0:T(8,128)(2,1)} %bitcast.13, bf16[2048,896]{1,0:T(8,128)(2,1)} %bitcast.14), custom_call_target="tpu_custom_call" | custom-call | tf_op jit(solution)/shard_map/dispatch/pallas_call | solution.py:239
  97.9 0.0 copy-done
  97.9 0.0 copy-done.1
  97.9 0.0 copy-done.2
  97.9 1.0 copy.16.weight_ref
  98.9 0.0 copy-start.3
  98.9 76.9 %give_back.1 = f32[1024,256]{1,0:T(8,128)} custom-call(bf16[2304,896]{1,0:T(8,128)(2,1)} %dispatch.1.h_ref, bf16[896,2048]{1,0:T(8,128)(2,1)} %bitcast.15, s32[1024,4]{1,0:T(8,128)} %copy-done, f32[1024,4]{1,0:T(8,128)} %copy.16.weight_ref), custom_call_target="tpu_custom_call" | custom-call | tf_op jit(solution)/shard_map/give_back/pallas_call | solution.py:404
  175.9 2.0 %multiply_reduce_fusion = f32[1024]{0:T(1024)} fusion(f32[1024,256]{1,0:T(8,128)} %give_back.1), kind=kLoop, calls=%fused_computation.10 | loop fusion | flops 523264 | bytes 1052672 | tf_op jit(solution)/shard_map/reduce_sum | solution.py:453
  177.9 9.3 %exchange3.1 = f32[8,128]{1,0:T(8,128)} custom-call(f32[8,128]{1,0:T(8,128)} %bitcast.18), custom_call_target="tpu_custom_call" | custom-call | tf_op jit(solution)/shard_map/exchange3/pallas_call | solution.py:47
  187.2 0.7 rsqrt_bitcast_fusion
  187.9 0.0 copy-done.3
  187.9 2.2 %multiply_convert_fusion = bf16[1024,256]{1,0:T(8,128)(2,1)} fusion(f32[1024,256]{1,0:T(8,128)} %give_back.1, f32[256]{0:T(256)S(1)} %convert_element_type.26, f32[1024]{0:T(1024)S(1)} %rsqrt_bitcast_fusion), kind=kLoop, calls=%fused_computation.9 | loop fusion | flops 786432 | bytes 1577984 | tf_op jit(solution)/shard_map/convert_element_type | solution.py:455
  (2 shorter events, 0.0 us)
Async XLA Ops:
  1.7 96.2 %copy-start = (s32[1024,4]{1,0:T(8,128)}, s32[1024,4]{1,0:T(8,128)S(1)}, u32[]{:S(2)}) copy-start(s32[1024,4]{1,0:T(8,128)S(1)} %fusion.2.key_ref) | copy-start | bytes 49156
  16.4 81.4 %copy-start.1 = (s32[1024,2]{0,1:T(2,128)S(1)}, s32[1024,2]{0,1:T(2,128)}, u32[]{:S(2)}) copy-start(s32[1024,2]{0,1:T(2,128)} %param.10) | copy-start | bytes 24580
  16.5 81.4 %copy-start.2 = (f32[1024,2]{0,1:T(2,128)S(1)}, f32[1024,2]{0,1:T(2,128)}, u32[]{:S(2)}) copy-start(f32[1024,2]{0,1:T(2,128)} %param.11) | copy-start | bytes 24580
  98.9 88.9 %copy-start.3 = (bf16[256]{0:T(256)(128)(2,1)S(1)}, bf16[256]{0:T(256)(128)(2,1)}, u32[]{:S(2)}) copy-start(bf16[256]{0:T(256)(128)(2,1)} %param.15) | copy-start | bytes 1540
where the time goes:
time: 191 us; the launch traced here: 190 us
  Pallas kernels  176 us (92%)
  other arithmetic  10.9 us (6%)
  local copies, waits for them, and re-layouts  2.12 us (1%)
    pallas_call x1, Pallas kernels, dispatch(): pl.pallas_call(functools.partial(dispatch_kernel, groups, layers, cap, co...  81.4 us
    pallas_call x1, Pallas kernels, give_back(): pl.pallas_call(functools.partial(return_kernel, groups, layers, cap, cols...  76.9 us
    pallas_call x2, Pallas kernels, sum_over_tp(): pl.pallas_call(functools.partial(exchange_kernel, n), out_shape=jax.Shape...  18 us

commit v1 on v0

v1 whole, which is shorter than its diff:
```python
import functools

import jax
import jax.numpy as jnp
from jax import lax
from jax.experimental import pallas as pl
from jax.experimental.pallas import tpu as pltpu
from jax.sharding import PartitionSpec as P

epsilon = 1e-06
MESH = pl.DeviceIdType.MESH
DMA = pltpu.SemaphoreType.DMA
BF16 = jnp.bfloat16
F32 = jnp.float32
LANES = 128


def flip(a, m, size):
    total, bit = 0, 1
    while bit < size:
        total = total + (((a // bit) % 2 + (m // bit) % 2) % 2) * bit
        bit *= 2
    return total


def columns_of(values):
    rows = values.shape[0]
    if rows < LANES:
        values = jnp.concatenate([values, jnp.zeros((LANES - rows, LANES), values.dtype)], axis=0)
    return values.T


def fold(wide, nb):
    row = lax.broadcasted_iota(jnp.int32, (nb, LANES), 0)
    total = None
    for r in range(nb):
        part = jnp.broadcast_to(wide[:, r * LANES : (r + 1) * LANES], (nb, LANES))
        total = part if total is None else jnp.where(row == r, part, total)
    return total


def squares_of(v, nb):
    square = v * v
    high = square.astype(BF16)
    low = (square - high.astype(F32)).astype(BF16)
    ones = jnp.ones((nb, v.shape[1]), BF16)
    dims = (((1,), (1,)), ((), ()))
    wide = lax.dot_general(ones, high, dims, preferred_element_type=F32)
    wide += lax.dot_general(ones, low, dims, preferred_element_type=F32)
    return fold(wide, nb)


def layer_kernel(
    L, G, cap, tile,
    x_ref, pre_ref, post_ref, ids_ref, rw_ref, gate_ref, up_ref, down_ref, out_ref,
    zbuf, nbuf, obuf, piece, wbuf, acc, hbuf, dbuf, rbuf, rin, abuf, tbuf,
    stat, stat2, kbuf, kcol, wcol, scol,
    zs, zr, es, er, fs, ds, dr, ws, dl, dps, dpr, hs, hr, rs, rr, as_, ar, ys, yr, ss, sr, ts, tr,
):
    tok, cols = x_ref.shape
    nb = tok // LANES
    n = 2 * L
    units = gate_ref.shape[1]
    rows = G * cap
    far = G - 1
    me, g = lax.axis_index("tp"), lax.axis_index("ep")
    core, z = lax.rem(me, 2), me // 2
    partner = {"tp": me + 1 - 2 * core}
    inside = jnp.logical_and(z > 0, z < L - 1)
    inner = jnp.minimum(z, L - 1 - z)
    width = n * cols

    def order(s):
        near = jnp.where(s % 2 == 1, z - (s + 1) // 2, z + (s + 1) // 2)
        rest = jnp.where(2 * z > L - 1, z - (s - inner), z + (s - inner))
        return jnp.where(s <= 2 * inner, near, rest)

    def beside(b):
        return jnp.logical_or(b == z + 1, b == z - 1)

    def group_rows(e):
        return pl.ds(pl.multiple_of(e * cap, 16), cap)

    def remote(src, dst, send, recv, to):
        return pltpu.make_async_remote_copy(
            src_ref=src, dst_ref=dst, send_sem=send, recv_sem=recv, device_id=to, device_id_type=MESH
        )

    def at_z(to):
        return {"tp": to * 2 + core}

    def at_g(m):
        return {"ep": flip(g, m, G)}

    def w_load(s, i):
        ref = (gate_ref, up_ref)[i]
        depth = pl.ds(pl.multiple_of(order(s) * 2 * cols, LANES), 2 * cols)
        return pltpu.make_async_copy(ref.at[depth], wbuf.at[s % 2, i], ws.at[s % 2, i])

    def my_units(c):
        return pl.ds(pl.multiple_of(c * units, 16), units)

    def down_part(b, c):
        return down_ref.at[:, pl.ds(pl.multiple_of((b * 2 + c) * cols, LANES), cols)]

    def down_own(b):
        return pltpu.make_async_copy(down_part(b, core), dbuf.at[b, my_units(core)], dl.at[b])

    def down_push(b):
        return remote(
            down_part(b, 1 - core), dbuf.at[b, my_units(core)], dps.at[b], dpr.at[b], partner
        )

    def z_copy(b, side):
        return remote(zbuf.at[b], zbuf.at[b], zs.at[side, b], zr.at[b], at_z(z + 1 - 2 * side))

    def e_copy(b, m):
        return remote(
            obuf.at[b, m - 1], piece.at[core, b, group_rows(g)], es.at[b, m], er.at[b, m], at_g(m)
        )

    def f_copy(side):
        area = piece.at[core, z, group_rows(flip(g, far, G))]
        return remote(area, area, fs.at[side], er.at[z, far], at_z(z + 1 - 2 * side))

    def d_copy(b, m):
        area = piece.at[core, b, group_rows(flip(g, m, G))]
        return remote(area, area, ds.at[b, m], dr.at[b, m], partner)

    def h_copy(m):
        area = hbuf.at[core, group_rows(flip(g, m, G))]
        return remote(area, area, hs.at[m], hr.at[m], partner)

    def r_copy(b, m):
        return remote(
            obuf.at[b, m - 1], rbuf.at[b, group_rows(g)], rs.at[b, m], rr.at[b, m], at_g(m)
        )

    def a_copy(b, side):
        return remote(obuf.at[b, far - 1], abuf.at[side], as_.at[side], ar.at[side], at_z(z + 1 - 2 * side))

    def y_copy(b, side):
        to = z + 1 - 2 * side
        slot = jnp.where(jnp.logical_and(to == b, side == 1), L, b)
        return remote(zbuf.at[b], rin.at[slot], ys.at[b], yr.at[slot], at_z(to))

    def stat_copy(buf, send, recv, k):
        to = lax.rem(me + k, n)
        return remote(buf.at[me], buf.at[me], send.at[to], recv.at[me], {"tp": to})

    def stat_wait(buf, send, recv, k):
        of = lax.rem(me + n - k, n)
        remote(buf.at[of], buf.at[of], send.at[of], recv.at[of], {"tp": of}).wait_recv()

    barrier = pltpu.get_barrier_semaphore()
    for k in range(1, n):
        pl.semaphore_signal(barrier, inc=1, device_id={"tp": lax.rem(me + k, n)}, device_id_type=MESH)
    for m in range(1, G):
        pl.semaphore_signal(barrier, inc=1, device_id=at_g(m), device_id_type=MESH)
    for s in range(2):
        for i in range(2):
            w_load(s, i).start()

    @pl.loop(0, L)
    def _(b):
        down_own(b).start()

    zbuf[z] = x_ref[...]
    stat[me, 0:nb] = squares_of(x_ref[...].astype(F32), nb)
    for c in range(cols // LANES):
        stat[me, nb + c : nb + c + 1] = pre_ref[:, c * LANES : (c + 1) * LANES].astype(F32)

    pl.semaphore_wait(barrier, n + G - 2)
    for k in range(1, n):
        stat_copy(stat, ss, sr, k).start()
    pl.when(z < L - 1)(z_copy(z, 0).start)
    pl.when(z > 0)(z_copy(z, 1).start)

    ids, weights = ids_ref[...], rw_ref[...]
    top = ids.shape[0]
    id_rows = [fold(ids[t : t + 1], nb) for t in range(top)]
    weight_rows = [fold(weights[t : t + 1], nb) for t in range(top)]
    members, shares = [], []
    for e in range(G):
        named = [r == e for r in id_rows]
        members.append(sum(jnp.where(q, 1.0, 0.0) for q in named))
        shares.append(sum(jnp.where(q, w, 0.0) for q, w in zip(named, weight_rows)))
    member = jnp.concatenate(members, axis=0)
    small = member.astype(BF16)
    lane_a = lax.broadcasted_iota(jnp.int32, (LANES, LANES), 0)
    lane_b = lax.broadcasted_iota(jnp.int32, (LANES, LANES), 1)
    both = jnp.concatenate(
        [jnp.where(lane_a < lane_b, 1.0, 0.0).astype(BF16), jnp.ones((LANES, LANES), BF16)], axis=1
    )
    counted = jnp.dot(small, both, preferred_element_type=F32)
    row_a = lax.broadcasted_iota(jnp.int32, (G * nb, G * nb), 0)
    row_b = lax.broadcasted_iota(jnp.int32, (G * nb, G * nb), 1)
    ahead = jnp.where(jnp.logical_and(row_a // nb == row_b // nb, row_b < row_a), 1.0, 0.0).astype(BF16)
    rank = counted[:, :LANES] + jnp.dot(
        ahead, counted[:, LANES:].astype(BF16), preferred_element_type=F32
    )
    base = (lax.broadcasted_iota(jnp.int32, (G * nb, LANES), 0) // nb * cap).astype(F32)
    key = jnp.where(member > 0.5, rank + base, -1.0)
    kbuf[...] = key.astype(jnp.int32)
    kcol[...] = columns_of(key).astype(jnp.int32)
    wcol[...] = columns_of(jnp.concatenate(shares, axis=0))

    for e in range(G):
        wanted = lax.broadcasted_iota(jnp.int32, (cap, LANES), 0) + e * cap
        for r in range(nb):
            l, lane = r * LANES // cols, r * LANES % cols
            rbuf[l, e * cap : (e + 1) * cap, lane : lane + LANES] = jnp.where(
                kbuf[e * nb + r : e * nb + r + 1] == wanted, 1.0, 0.0
            ).astype(BF16)

    def row_scale(buf, send, recv):
        for k in range(1, n):
            stat_wait(buf, send, recv, k)
        total = buf[0, 0:nb]
        for k in range(1, n):
            total = total + buf[k, 0:nb]
        return columns_of(lax.rsqrt(total / width + epsilon))

    scol[...] = row_scale(stat, ss, sr)

    @pl.loop(0, L)
    def _(b):
        down_push(b).start()

    def take(s):
        b = order(s)
        z_copy(b, 0).wait_recv()
        pl.when(jnp.logical_and(b < z, z < L - 1))(z_copy(b, 0).start)
        pl.when(jnp.logical_and(b > z, z > 0))(z_copy(b, 1).start)

    def process(s):
        b = order(s)
        gain = jnp.concatenate(
            [stat[b * 2 + core, nb + c : nb + c + 1] for c in range(cols // LANES)], axis=1
        )
        for r in range(nb):
            at = slice(r * LANES, (r + 1) * LANES)
            nbuf[at] = (zbuf[b, at].astype(F32) * scol[:, r : r + 1] * gain).astype(BF16)

        @pl.loop(0, G)
        def _(j):
            m = G - 1 - j

            @pl.when(jnp.logical_not(jnp.logical_and(m == far, beside(b))))
            def _():
                at = group_rows(flip(g, m, G))
                chooser = jnp.concatenate([rbuf[l, at] for l in range(tok // cols)], axis=1)
                chosen = jnp.dot(chooser, nbuf[...], preferred_element_type=F32).astype(BF16)

                @pl.when(m > 0)
                def _():
                    obuf[b, m - 1] = chosen
                    e_copy(b, m).start()

                @pl.when(m == 0)
                def _():
                    piece[core, b, group_rows(g)] = chosen
                    d_copy(b, 0).start()

    def gate_up(b, slot, at):
        left = jnp.concatenate([piece[0, b, at], piece[1, b, at]], axis=1)
        return [jnp.dot(left, wbuf[slot, i], preferred_element_type=F32) for i in range(2)]

    def finish(s):
        b, slot = order(s), s % 2

        @pl.loop(1, G)
        def _(j):
            m = G - j
            e_copy(b, m).wait_recv()

            @pl.when(jnp.logical_and(m == far, b == z))
            def _():
                pl.when(z < L - 1)(f_copy(0).start)
                pl.when(z > 0)(f_copy(1).start)

            d_copy(b, m).start()

        @pl.loop(0, G)
        def _(m):
            d_copy(b, m).wait_recv()

        for i in range(2):
            w_load(s, i).wait()

        @pl.loop(0, rows // tile)
        def _(t):
            at = pl.ds(pl.multiple_of(t * tile, 16), tile)
            both = gate_up(b, slot, at)

            @pl.when(s == 0)
            def _():
                for i in range(2):
                    acc[i, at] = both[i]

            @pl.when(s > 0)
            def _():
                for i in range(2):
                    acc[i, at] += both[i]

        @pl.when(s + 2 < L)
        def _():
            for i in range(2):
                w_load(s + 2, i).start()

    process(0)

    @pl.loop(1, L)
    def _(s):
        pl.when(jnp.logical_or(jnp.logical_not(inside), s == 1))(lambda: take(s))
        process(s)
        pl.when(jnp.logical_and(inside, s + 1 < L))(lambda: take(s + 1))
        finish(s - 1)

    def project(i, m):
        b = order(L - 1 - i)
        at = group_rows(flip(g, m, G))
        if units % LANES == 0:
            left = jnp.concatenate([hbuf[0, at], hbuf[1, at]], axis=1)
            result = jnp.dot(left, dbuf[b], preferred_element_type=F32)
        else:
            result = jnp.dot(hbuf[0, at], dbuf[b, 0:units], preferred_element_type=F32)
            result += jnp.dot(hbuf[1, at], dbuf[b, units:], preferred_element_type=F32)

        @pl.when(m == 0)
        def _():
            rbuf[b, at] = result.astype(BF16)

        @pl.when(jnp.logical_and(m > 0, m < far))
        def _():
            e_copy(b, m).wait_send()
            obuf[b, m - 1] = result.astype(BF16)
            r_copy(b, m).start()

        @pl.when(m == far)
        def _():
            @pl.when(beside(b))
            def _():
                obuf[b, far - 1] = result.astype(BF16)
                pl.when(b > z)(a_copy(b, 0).start)
                pl.when(b < z)(a_copy(b, 1).start)

            @pl.when(jnp.logical_not(beside(b)))
            def _():
                e_copy(b, far).wait_send()

                @pl.when(b == z)
                def _():
                    tbuf[0:cap] = result

                    @pl.when(z > 0)
                    def _():
                        a_copy(b, 0).wait_recv()
                        tbuf[0:cap] += abuf[0].astype(F32)

                    @pl.when(z < L - 1)
                    def _():
                        a_copy(b, 1).wait_recv()
                        tbuf[0:cap] += abuf[1].astype(F32)

                    obuf[b, far - 1] = tbuf[0:cap].astype(BF16)

                @pl.when(b != z)
                def _():
                    obuf[b, far - 1] = result.astype(BF16)

                r_copy(b, far).start()

    def down_ready(b):
        down_own(b).wait()
        down_push(b).wait_recv()

    last = order(L - 1)
    for i in range(2):
        w_load(L - 1, i).wait()
    down_ready(last)

    @pl.loop(0, G + 1)
    def _(m):
        @pl.when(jnp.logical_and(m > 0, m < G))
        def _():
            e_copy(last, m).wait_recv()
            d_copy(last, m).start()

        @pl.when(m > 0)
        def _():
            h_copy(m - 1).wait_recv()
            project(0, m - 1)

        @pl.when(m < G)
        def _():
            d_copy(last, m).wait_recv()
            first = flip(g, m, G) * cap

            @pl.loop(0, cap // tile)
            def _(t):
                at = pl.ds(pl.multiple_of(first + t * tile, 16), tile)
                both = gate_up(last, (L - 1) % 2, at)
                gates = acc[0, at] + both[0]
                half = 0.5 * gates
                hbuf[core, at] = ((half + half * jnp.tanh(half)) * (acc[1, at] + both[1])).astype(BF16)

            h_copy(m).start()

    @pl.loop(1, L)
    def _(i):
        b = order(L - 1 - i)
        down_ready(b)

        @pl.loop(0, G)
        def _(j):
            project(i, jnp.where(i == L - 1, j, G - 1 - j))

    pl.when(z < L - 1)(z_copy(z, 0).wait_send)
    pl.when(z > 0)(z_copy(z, 1).wait_send)
    pl.when(z < L - 1)(f_copy(0).wait_send)
    pl.when(z > 0)(f_copy(1).wait_send)

    @pl.loop(0, L)
    def _(b):
        pl.when(jnp.logical_and(b < z, z < L - 1))(z_copy(b, 0).wait_send)
        pl.when(jnp.logical_and(b > z, z > 0))(z_copy(b, 1).wait_send)

        @pl.loop(0, G)
        def _(m):
            d_copy(b, m).wait_send()

        @pl.when(beside(b))
        def _():
            rbuf[b, group_rows(flip(g, far, G))] = jnp.zeros((cap, cols), BF16)

    per = rows // tok
    blocks = rows // cols

    def mix_place(k):
        return k // (L * per), (k // per) % L, (k % per) * tok

    for k in range(blocks):
        c, b, first = mix_place(k)
        lane = lax.broadcasted_iota(jnp.int32, (LANES, cols), 1) + k * cols
        for r in range(nb):
            value = jnp.zeros((LANES, cols), F32)
            for e in range(k * cols // cap, ((k + 1) * cols - 1) // cap + 1):
                q = e * nb + r
                value = jnp.where(kcol[:, q : q + 1] == lane, wcol[:, q : q + 1], value)
            piece[c, b, first + r * LANES : first + (r + 1) * LANES] = value.astype(BF16)

    step = min(256, tok)

    def combined(b, t):
        parts = []
        for k in range(blocks):
            c, l, first = mix_place(k)
            parts.append(piece[c, l, pl.ds(pl.multiple_of(first + t * step, 16), step)])
        return jnp.dot(jnp.concatenate(parts, axis=1), rbuf[b], preferred_element_type=F32)

    def arrived(b):
        @pl.loop(1, G)
        def _(m):
            @pl.when(jnp.logical_not(jnp.logical_and(m == far, beside(b))))
            def _():
                r_copy(b, m).wait_recv()

    @pl.loop(0, L - 1)
    def _(i):
        b = order(L - 1 - i)
        more = jnp.where(b > z, z, L - 1 - z) > 0
        arrived(b)

        @pl.when(more)
        def _():
            remote(zbuf.at[b], rin.at[b], ys.at[b], yr.at[b], at_z(b)).wait_recv()

        @pl.loop(0, tok // step)
        def _(t):
            at = pl.ds(pl.multiple_of(t * step, 16), step)
            value = combined(b, t)

            @pl.when(more)
            def _():
                zbuf[b, at] = (value + rin[b, at].astype(F32)).astype(BF16)

            @pl.when(jnp.logical_not(more))
            def _():
                zbuf[b, at] = value.astype(BF16)

        pl.when(b > z)(y_copy(b, 0).start)
        pl.when(b < z)(y_copy(b, 1).start)

    arrived(z)

    @pl.loop(0, tok // step)
    def _(t):
        at = pl.ds(pl.multiple_of(t * step, 16), step)
        tbuf[at] = combined(z, t)

    for side, slot in ((0, z), (1, L)):
        @pl.when(z > 0 if side == 0 else z < L - 1)
        def _():
            remote(zbuf.at[z], rin.at[slot], ys.at[z], yr.at[slot], partner).wait_recv()
            tbuf[...] += rin[slot].astype(F32)

    stat2[me] = squares_of(tbuf[...], nb)
    for k in range(1, n):
        stat_copy(stat2, ts, tr, k).start()
    post = post_ref[...].astype(F32)
    scol[...] = row_scale(stat2, ts, tr)
    for r in range(nb):
        at = slice(r * LANES, (r + 1) * LANES)
        out_ref[at] = (tbuf[at] * scol[:, r : r + 1] * post).astype(BF16)

    for k in range(1, n):
        stat_copy(stat, ss, sr, k).wait_send()
        stat_copy(stat2, ts, tr, k).wait_send()

    pl.when(z < L - 1)(a_copy(z + 1, 0).wait_send)
    pl.when(z > 0)(a_copy(z - 1, 1).wait_send)

    @pl.loop(0, L)
    def _(b):
        down_push(b).wait_send()
        pl.when(b > z)(y_copy(b, 0).wait_send)
        pl.when(b < z)(y_copy(b, 1).wait_send)

        @pl.loop(1, G)
        def _(m):
            @pl.when(jnp.logical_not(jnp.logical_and(m == far, beside(b))))
            def _():
                r_copy(b, m).wait_send()

    @pl.loop(0, G)
    def _(m):
        h_copy(m).wait_send()


def on_device(
    tokens, pre_gain, route_ids, route_weights, gate_weight, up_weight, down_weight, post_gain
):
    tok, cols = tokens.shape
    top = route_ids.shape[1]
    G = lax.axis_size("ep")
    n = lax.axis_size("tp")
    L = n // 2
    cap = 9 * tok * top // (8 * G)
    rows = G * cap
    units = gate_weight.shape[2]
    nb = tok // LANES
    tile = cap
    vmem = pl.BlockSpec(memory_space=pltpu.VMEM)
    hbm = pl.BlockSpec(memory_space=pl.ANY)
    return pl.pallas_call(
        functools.partial(layer_kernel, L, G, cap, tile),
        out_shape=jax.ShapeDtypeStruct((tok, cols), BF16),
        in_specs=[vmem] * 5 + [hbm] * 3,
        out_specs=vmem,
        scratch_shapes=[
            pltpu.VMEM((L, tok, cols), BF16),
            pltpu.VMEM((tok, cols), BF16),
            pltpu.VMEM((L, G - 1, cap, cols), BF16),
            pltpu.VMEM((2, L, rows, cols), BF16),
            pltpu.VMEM((2, 2, 2 * cols, units), BF16),
            pltpu.VMEM((2, rows, units), F32),
            pltpu.VMEM((2, rows, units), BF16),
            pltpu.VMEM((L, 2 * units, cols), BF16),
            pltpu.VMEM((L, rows, cols), BF16),
            pltpu.VMEM((L + 1, tok, cols), BF16),
            pltpu.VMEM((2, cap, cols), BF16),
            pltpu.VMEM((tok, cols), F32),
            pltpu.VMEM((n, 2 * nb, LANES), F32),
            pltpu.VMEM((n, nb, LANES), F32),
            pltpu.VMEM((G * nb, LANES), jnp.int32),
            pltpu.VMEM((LANES, LANES), jnp.int32),
            pltpu.VMEM((LANES, LANES), F32),
            pltpu.VMEM((LANES, LANES), F32),
            DMA((2, L)), DMA((L,)),
            DMA((L, G)), DMA((L, G)),
            DMA((2,)),
            DMA((L, G)), DMA((L, G)),
            DMA((2, 2)),
            DMA((L,)), DMA((L,)), DMA((L,)),
            DMA((G,)), DMA((G,)),
            DMA((L, G)), DMA((L, G)),
            DMA((2,)), DMA((2,)),
            DMA((L,)), DMA((L + 1,)),
            DMA((n,)), DMA((n,)),
            DMA((n,)), DMA((n,)),
        ],
        compiler_params=pltpu.CompilerParams(
            collective_id=1, has_side_effects=True, vmem_limit_bytes=62 * 2**20
        ),
        name="layer",
    )(
        tokens, pre_gain.reshape(1, cols), post_gain.reshape(1, cols), route_ids.T, route_weights.T,
        gate_weight[0], up_weight[0], down_weight[0],
    )


def solution(mesh):
    placed = (
        P("ep", "tp"),
        P("tp"),
        P("ep", None),
        P("ep", None),
        P("ep", None, "tp"),
        P("ep", None, "tp"),
        P("ep", "tp", None),
        P("tp"),
    )
    return jax.shard_map(
        on_device, mesh=mesh, in_specs=placed, out_specs=P("ep", "tp"), check_vma=False
    )
```

time: 191 us -> 152 us (0.80)
  Pallas kernels: 176 us -> 147 us
  other arithmetic: 10.9 us -> 0 us
  local copies, waits for them, and re-layouts: 2.12 us -> 4.34 us
    pallas_call x4 -> x1, Pallas kernels: 176 us -> 147 us  [on_device(): pl.pallas_call(functools.partial(layer_kernel, L, G, cap, tile), out_shap...]
    convert_element_type x4 -> x0, other arithmetic: 4.93 us -> none  [the longest x2 2.23 us: on_device(): return (scaled * post_gain.astype(jnp.float32)[None, :]).astype(BF16)]
    reduce_sum x3 -> x0, other arithmetic: 3.9 us -> none  [the longest x1 2.03 us: on_device(): totals = sum_over_tp(jnp.sum(combined * combined, axis=1), 3)]
where the time goes in v1:
time: 152 us; the launch traced here: 151 us
  Pallas kernels  147 us (97%)
  local copies, waits for them, and re-layouts  4.34 us (3%)
    pallas_call x1, Pallas kernels, on_device(): pl.pallas_call(functools.partial(layer_kernel, L, G, cap, tile), out_shap...  147 us

profile of v1, /device:TPU:0, one launch (start us, length us, event | category | flops | bytes accessed | tf_op | source)
XLA Modules:
  0.0 151.4 jit_solution(10571962916186181505)
XLA Ops:
  0.0 1.2 reshape.6.pre_ref
  1.2 1.2 reshape.7.post_ref
  2.5 147.0 %layer.1 = bf16[1024,256]{1,0:T(8,128)(2,1)} custom-call(bf16[1024,256]{1,0:T(8,128)(2,1)} %x_ref.1, bf16[1,256]{1,0:T(2,128)(2,1)} %reshape.6.pre_ref, bf16[1,256]{1,0:T(2,128)(2,1)} %reshape.7.post_ref, s32[2,1024]{1,0:T(2,128)} %bitcast.8, f32[2,1024]{1,0:T(2,128)} %bitcast.9, bf16[2048,896]{1,0:T(8,128)(2,1)} %bitcast.5, bf16[2048,896]{1,0:T(8,128)(2,1)} %bitcast.6, ...), custom_call_target="tpu_custom_call" | custom-call | tf_op jit(solution)/shard_map/layer/pallas_call | solution.py:556
  149.5 1.9 %copy.10 = bf16[1024,256]{1,0:T(8,128)(2,1)} copy(bf16[1024,256]{1,0:T(8,128)(2,1)} %layer.1) | data formatting | bytes 1048576

commit v2 on v1

--- a/solution.py
+++ b/solution.py
@@ -55,9 +55,9 @@
     x_ref, pre_ref, post_ref, ids_ref, rw_ref, gate_ref, up_ref, down_ref, out_ref,
     zbuf, nbuf, obuf, piece, wbuf, acc, hbuf, dbuf, rbuf, rin, abuf, tbuf,
     stat, stat2, kbuf, kcol, wcol, scol,
-    zs, zr, es, er, fs, ds, dr, ws, dl, dps, dpr, hs, hr, rs, rr, as_, ar, ys, yr, ss, sr, ts, tr,
+    zs, zr, es, er, fs, ds, dr, ws, dl, dps, dpr, hs, hr, rs, rr, as_, ar, ys, yr, ss, sr, ts, tr, xs,
 ):
-    tok, cols = x_ref.shape
+    tok, cols = nbuf.shape
     nb = tok // LANES
     n = 2 * L
     units = gate_ref.shape[1]
@@ -75,8 +75,13 @@
         rest = jnp.where(2 * z > L - 1, z - (s - inner), z + (s - inner))
         return jnp.where(s <= 2 * inner, near, rest)
 
-    def beside(b):
-        return jnp.logical_or(b == z + 1, b == z - 1)
+    farthest = jnp.where(2 * z > L - 1, 0, L - 1)
+    end_left = z == 1
+    next_to_end = jnp.logical_or(z == 1, z == L - 2)
+
+    def skipped(b):
+        beside = jnp.logical_or(b == z + 1, b == z - 1)
+        return jnp.where(inside, beside, b == farthest)
 
     def group_rows(e):
         return pl.ds(pl.multiple_of(e * cap, 16), cap)
@@ -122,6 +127,10 @@
     def f_copy(side):
         area = piece.at[core, z, group_rows(flip(g, far, G))]
         return remote(area, area, fs.at[side], er.at[z, far], at_z(z + 1 - 2 * side))
+
+    def l_copy():
+        area = piece.at[core, farthest, group_rows(flip(g, far, G))]
+        return remote(area, area, fs.at[2], er.at[farthest, far], at_z(jnp.where(end_left, 0, L - 1)))
 
     def d_copy(b, m):
         area = piece.at[core, b, group_rows(flip(g, m, G))]
@@ -157,6 +166,8 @@
         pl.semaphore_signal(barrier, inc=1, device_id={"tp": lax.rem(me + k, n)}, device_id_type=MESH)
     for m in range(1, G):
         pl.semaphore_signal(barrier, inc=1, device_id=at_g(m), device_id_type=MESH)
+    x_load = pltpu.make_async_copy(x_ref, zbuf.at[z], xs.at[0])
+    x_load.start()
     for s in range(2):
         for i in range(2):
             w_load(s, i).start()
@@ -165,10 +176,11 @@
     def _(b):
         down_own(b).start()
 
-    zbuf[z] = x_ref[...]
-    stat[me, 0:nb] = squares_of(x_ref[...].astype(F32), nb)
+    x_load.wait()
+    stat[me, 0:nb] = squares_of(zbuf[z].astype(F32), nb)
+    pre = pre_ref[...].astype(F32).reshape(1, cols)
     for c in range(cols // LANES):
-        stat[me, nb + c : nb + c + 1] = pre_ref[:, c * LANES : (c + 1) * LANES].astype(F32)
+        stat[me, nb + c : nb + c + 1] = pre[:, c * LANES : (c + 1) * LANES]
 
     pl.semaphore_wait(barrier, n + G - 2)
     for k in range(1, n):
@@ -246,7 +258,7 @@
         def _(j):
             m = G - 1 - j
 
-            @pl.when(jnp.logical_not(jnp.logical_and(m == far, beside(b))))
+            @pl.when(jnp.logical_not(jnp.logical_and(m == far, skipped(b))))
             def _():
                 at = group_rows(flip(g, m, G))
                 chooser = jnp.concatenate([rbuf[l, at] for l in range(tok // cols)], axis=1)
@@ -276,8 +288,8 @@
 
             @pl.when(jnp.logical_and(m == far, b == z))
             def _():
-                pl.when(z < L - 1)(f_copy(0).start)
-                pl.when(z > 0)(f_copy(1).start)
+                pl.when(z < L - 2)(f_copy(0).start)
+                pl.when(z > 1)(f_copy(1).start)
 
             d_copy(b, m).start()
 
@@ -312,10 +324,37 @@
 
     @pl.loop(1, L)
     def _(s):
-        pl.when(jnp.logical_or(jnp.logical_not(inside), s == 1))(lambda: take(s))
-        process(s)
-        pl.when(jnp.logical_and(inside, s + 1 < L))(lambda: take(s + 1))
+        @pl.when(jnp.logical_or(jnp.logical_not(inside), s == 1))
+        def _():
+            take(s)
+            pl.when(inside)(lambda: take(s + 1))
+            process(s)
+
+        @pl.when(jnp.logical_and(inside, s + 1 < L))
+        def _():
+            pl.when(s > 1)(lambda: take(s + 1))
+            process(s + 1)
+
+        @pl.when(jnp.logical_and(next_to_end, s == L - 1))
+        def _():
+            e_copy(farthest, far).wait_recv()
+            l_copy().start()
+
         finish(s - 1)
+
+    def extra(b, side):
+        if side == 0:
+            return jnp.logical_and(z > 0, b == jnp.where(z > 1, z, L - 1))
+        return jnp.logical_and(z < L - 1, b == jnp.where(z < L - 2, z, 0))
+
+    def add_extra(b):
+        for side in range(2):
+            @pl.when(extra(b, side))
+            def _():
+                a_copy(b, side).wait_recv()
+                tbuf[0:cap] += abuf[side].astype(F32)
+
+        obuf[b, far - 1] = tbuf[0:cap].astype(BF16)
 
     def project(i, m):
         b = order(L - 1 - i)
@@ -335,65 +374,72 @@
         def _():
             e_copy(b, m).wait_send()
             obuf[b, m - 1] = result.astype(BF16)
-            r_copy(b, m).start()
 
         @pl.when(m == far)
         def _():
-            @pl.when(beside(b))
+            @pl.when(skipped(b))
             def _():
                 obuf[b, far - 1] = result.astype(BF16)
-                pl.when(b > z)(a_copy(b, 0).start)
-                pl.when(b < z)(a_copy(b, 1).start)
-
-            @pl.when(jnp.logical_not(beside(b)))
+                to_right = jnp.where(inside, b > z, z == 0)
+                pl.when(to_right)(a_copy(b, 0).start)
+                pl.when(jnp.logical_not(to_right))(a_copy(b, 1).start)
+
+            @pl.when(jnp.logical_not(skipped(b)))
             def _():
                 e_copy(b, far).wait_send()
-
-                @pl.when(b == z)
+                tbuf[0:cap] = result
+
+                @pl.when(i > 0)
                 def _():
-                    tbuf[0:cap] = result
-
-                    @pl.when(z > 0)
-                    def _():
-                        a_copy(b, 0).wait_recv()
-                        tbuf[0:cap] += abuf[0].astype(F32)
-
-                    @pl.when(z < L - 1)
-                    def _():
-                        a_copy(b, 1).wait_recv()
-                        tbuf[0:cap] += abuf[1].astype(F32)
-
-                    obuf[b, far - 1] = tbuf[0:cap].astype(BF16)
-
-                @pl.when(b != z)
-                def _():
-                    obuf[b, far - 1] = result.astype(BF16)
-
-                r_copy(b, far).start()
+                    add_extra(b)
+
+    def each_send(i, act):
+        b = order(L - 1 - i)
+
+        @pl.loop(0, G - 1)
+        def _(j):
+            m = far - j
+
+            @pl.when(jnp.logical_not(jnp.logical_and(m == far, skipped(b))))
+            def _():
+                act(b, m)
+
+    def start_sends(i):
+        each_send(i, lambda b, m: r_copy(b, m).start())
+
+    def wait_sends(i):
+        each_send(i, lambda b, m: r_copy(b, m).wait_send())
 
     def down_ready(b):
         down_own(b).wait()
         down_push(b).wait_recv()
 
+    def project_all(i):
+        down_ready(order(L - 1 - i))
+
+        @pl.loop(0, G)
+        def _(j):
+            project(i, G - 1 - j)
+
     last = order(L - 1)
+
+    @pl.loop(1, G)
+    def _(m):
+        @pl.when(jnp.logical_not(jnp.logical_and(m == far, next_to_end)))
+        def _():
+            e_copy(last, m).wait_recv()
+
+        d_copy(last, m).start()
+
     for i in range(2):
         w_load(L - 1, i).wait()
     down_ready(last)
 
     @pl.loop(0, G + 1)
-    def _(m):
-        @pl.when(jnp.logical_and(m > 0, m < G))
-        def _():
-            e_copy(last, m).wait_recv()
-            d_copy(last, m).start()
-
-        @pl.when(m > 0)
-        def _():
-            h_copy(m - 1).wait_recv()
-            project(0, m - 1)
-
-        @pl.when(m < G)
-        def _():
+    def _(q):
+        @pl.when(q < G)
+        def _():
+            m = lax.rem(q + 1, G)
             d_copy(last, m).wait_recv()
             first = flip(g, m, G) * cap
 
@@ -407,19 +453,33 @@
 
             h_copy(m).start()
 
-    @pl.loop(1, L)
-    def _(i):
-        b = order(L - 1 - i)
-        down_ready(b)
-
-        @pl.loop(0, G)
-        def _(j):
-            project(i, jnp.where(i == L - 1, j, G - 1 - j))
+        @pl.when(q > 0)
+        def _():
+            m = lax.rem(q, G)
+            h_copy(m).wait_recv()
+            project(0, m)
+            direct = jnp.logical_and(m > 0, m < far)
+            pl.when(direct)(lambda: r_copy(last, m).start())
+
+            @pl.when(jnp.logical_and(m == far, jnp.logical_not(jnp.logical_or(skipped(last), next_to_end))))
+            def _():
+                obuf[last, far - 1] = tbuf[0:cap].astype(BF16)
+                r_copy(last, far).start()
+
+    @pl.when(next_to_end)
+    def _():
+        add_extra(last)
+        r_copy(last, far).start()
+
+    project_all(1)
+    wait_sends(0)
+    start_sends(1)
 
     pl.when(z < L - 1)(z_copy(z, 0).wait_send)
     pl.when(z > 0)(z_copy(z, 1).wait_send)
-    pl.when(z < L - 1)(f_copy(0).wait_send)
-    pl.when(z > 0)(f_copy(1).wait_send)
+    pl.when(z < L - 2)(f_copy(0).wait_send)
+    pl.when(z > 1)(f_copy(1).wait_send)
+    pl.when(next_to_end)(l_copy().wait_send)
 
     @pl.loop(0, L)
     def _(b):
@@ -430,7 +490,7 @@
         def _(m):
             d_copy(b, m).wait_send()
 
-        @pl.when(beside(b))
+        @pl.when(skipped(b))
         def _():
             rbuf[b, group_rows(flip(g, far, G))] = jnp.zeros((cap, cols), BF16)
 
@@ -462,12 +522,18 @@
     def arrived(b):
         @pl.loop(1, G)
         def _(m):
-            @pl.when(jnp.logical_not(jnp.logical_and(m == far, beside(b))))
+            @pl.when(jnp.logical_not(jnp.logical_and(m == far, skipped(b))))
             def _():
                 r_copy(b, m).wait_recv()
 
     @pl.loop(0, L - 1)
     def _(i):
+        @pl.when(i > 0)
+        def _():
+            wait_sends(i)
+            start_sends(i + 1)
+
+        pl.when(i + 2 < L)(lambda: project_all(i + 2))
         b = order(L - 1 - i)
         more = jnp.where(b > z, z, L - 1 - z) > 0
         arrived(b)
@@ -508,18 +574,27 @@
     stat2[me] = squares_of(tbuf[...], nb)
     for k in range(1, n):
         stat_copy(stat2, ts, tr, k).start()
-    post = post_ref[...].astype(F32)
+    post = post_ref[...].astype(F32).reshape(1, cols)
     scol[...] = row_scale(stat2, ts, tr)
     for r in range(nb):
         at = slice(r * LANES, (r + 1) * LANES)
-        out_ref[at] = (tbuf[at] * scol[:, r : r + 1] * post).astype(BF16)
+        nbuf[at] = (tbuf[at] * scol[:, r : r + 1] * post).astype(BF16)
+    out_copy = pltpu.make_async_copy(nbuf, out_ref, xs.at[0])
+    out_copy.start()
 
     for k in range(1, n):
         stat_copy(stat, ss, sr, k).wait_send()
         stat_copy(stat2, ts, tr, k).wait_send()
 
-    pl.when(z < L - 1)(a_copy(z + 1, 0).wait_send)
-    pl.when(z > 0)(a_copy(z - 1, 1).wait_send)
+    pl.when(z == 0)(a_copy(farthest, 0).wait_send)
+    pl.when(z == L - 1)(a_copy(farthest, 1).wait_send)
+
+    @pl.when(inside)
+    def _():
+        a_copy(z + 1, 0).wait_send()
+        a_copy(z - 1, 1).wait_send()
+
+    wait_sends(L - 1)
 
     @pl.loop(0, L)
     def _(b):
@@ -527,15 +602,11 @@
         pl.when(b > z)(y_copy(b, 0).wait_send)
         pl.when(b < z)(y_copy(b, 1).wait_send)
 
-        @pl.loop(1, G)
-        def _(m):
-            @pl.when(jnp.logical_not(jnp.logical_and(m == far, beside(b))))
-            def _():
-                r_copy(b, m).wait_send()
-
     @pl.loop(0, G)
     def _(m):
         h_copy(m).wait_send()
+
+    out_copy.wait()
 
 
 def on_device(
@@ -556,8 +627,8 @@
     return pl.pallas_call(
         functools.partial(layer_kernel, L, G, cap, tile),
         out_shape=jax.ShapeDtypeStruct((tok, cols), BF16),
-        in_specs=[vmem] * 5 + [hbm] * 3,
-        out_specs=vmem,
+        in_specs=[hbm] + [vmem] * 4 + [hbm] * 3,
+        out_specs=hbm,
         scratch_shapes=[
             pltpu.VMEM((L, tok, cols), BF16),
             pltpu.VMEM((tok, cols), BF16),
@@ -579,7 +650,7 @@
             pltpu.VMEM((LANES, LANES), F32),
             DMA((2, L)), DMA((L,)),
             DMA((L, G)), DMA((L, G)),
-            DMA((2,)),
+            DMA((3,)),
             DMA((L, G)), DMA((L, G)),
             DMA((2, 2)),
             DMA((L,)), DMA((L,)), DMA((L,)),
@@ -589,13 +660,14 @@
             DMA((L,)), DMA((L + 1,)),
             DMA((n,)), DMA((n,)),
             DMA((n,)), DMA((n,)),
+            DMA((1,)),
         ],
         compiler_params=pltpu.CompilerParams(
             collective_id=1, has_side_effects=True, vmem_limit_bytes=62 * 2**20
         ),
         name="layer",
     )(
-        tokens, pre_gain.reshape(1, cols), post_gain.reshape(1, cols), route_ids.T, route_weights.T,
+        tokens, pre_gain, post_gain, route_ids.T, route_weights.T,
         gate_weight[0], up_weight[0], down_weight[0],
     )
 

time: 152 us -> 138 us (0.908)
  Pallas kernels: 147 us -> 136 us
  local copies, waits for them, and re-layouts: 4.34 us -> 1.87 us
    pallas_call x1, Pallas kernels: 147 us -> 136 us  [on_device(): pl.pallas_call(functools.partial(layer_kernel, L, G, cap, tile), out_shap...]
    reshape x2 -> x0, local copies, waits for them, and re-layouts: 2.47 us -> none  [the longest x1 1.25 us: on_device(): post_gain.reshape(1, cols)]
where the time goes in v2:
time: 138 us
  Pallas kernels  136 us (99%)
  local copies, waits for them, and re-layouts  1.87 us (1%)
    pallas_call x1, Pallas kernels, on_device(): pl.pallas_call(functools.partial(layer_kernel, L, G, cap, tile), out_shap...  136 us

profile of v2, /device:TPU:0, one launch (start us, length us, event | category | flops | bytes accessed | tf_op | source)
XLA Modules:
  0.0 138.2 jit_solution(10969193696970782602)
XLA Ops:
  0.0 136.4 %layer.1 = bf16[1024,256]{1,0:T(8,128)(2,1)} custom-call(bf16[1024,256]{1,0:T(8,128)(2,1)} %x_ref.1, bf16[256]{0:T(256)(128)(2,1)} %pre_ref.1, bf16[256]{0:T(256)(128)(2,1)} %post_ref.1, s32[2,1024]{1,0:T(2,128)} %bitcast.8, f32[2,1024]{1,0:T(2,128)} %bitcast.9, bf16[2048,896]{1,0:T(8,128)(2,1)} %bitcast.5, bf16[2048,896]{1,0:T(8,128)(2,1)} %bitcast.6, ...), custom_call_target="tpu_custom_call" | custom-call | tf_op jit(solution)/shard_map/layer/pallas_call | solution.py:627
  136.4 1.9 %copy.10 = bf16[1024,256]{1,0:T(8,128)(2,1)} copy(bf16[1024,256]{1,0:T(8,128)(2,1)} %layer.1) | data formatting | bytes 1048576

commit v3 on v2

--- a/solution.py
+++ b/solution.py
@@ -53,7 +53,7 @@
 def layer_kernel(
     L, G, cap, tile,
     x_ref, pre_ref, post_ref, ids_ref, rw_ref, gate_ref, up_ref, down_ref, out_ref,
-    zbuf, nbuf, obuf, piece, wbuf, acc, hbuf, dbuf, rbuf, rin, abuf, tbuf,
+    zbuf, nbuf, obuf, piece, wbuf, acc, hbuf, dbuf, rbuf, rin, abuf, ebuf, tbuf,
     stat, stat2, kbuf, kcol, wcol, scol,
     zs, zr, es, er, fs, ds, dr, ws, dl, dps, dpr, hs, hr, rs, rr, as_, ar, ys, yr, ss, sr, ts, tr, xs,
 ):
@@ -69,6 +69,8 @@
     inside = jnp.logical_and(z > 0, z < L - 1)
     inner = jnp.minimum(z, L - 1 - z)
     width = n * cols
+    step = min(256, tok)
+    tiles = tok // step
 
     def order(s):
         near = jnp.where(s % 2 == 1, z - (s + 1) // 2, z + (s + 1) // 2)
@@ -76,6 +78,7 @@
         return jnp.where(s <= 2 * inner, near, rest)
 
     farthest = jnp.where(2 * z > L - 1, 0, L - 1)
+    last = order(L - 1)
     end_left = z == 1
     next_to_end = jnp.logical_or(z == 1, z == L - 2)
 
@@ -148,10 +151,17 @@
     def a_copy(b, side):
         return remote(obuf.at[b, far - 1], abuf.at[side], as_.at[side], ar.at[side], at_z(z + 1 - 2 * side))
 
-    def y_copy(b, side):
+    def rows_of(t):
+        return pl.ds(pl.multiple_of(t * step, 16), step)
+
+    def y_copy(b, side, t):
         to = z + 1 - 2 * side
         slot = jnp.where(jnp.logical_and(to == b, side == 1), L, b)
-        return remote(zbuf.at[b], rin.at[slot], ys.at[b], yr.at[slot], at_z(to))
+        return remote(zbuf.at[b, rows_of(t)], rin.at[slot, rows_of(t)], ys.at[b, t], yr.at[slot, t], at_z(to))
+
+    def y_wait(slot, t):
+        area = rin.at[slot, rows_of(t)]
+        remote(area, area, ys.at[0, t], yr.at[slot, t], partner).wait_recv()
 
     def stat_copy(buf, send, recv, k):
         to = lax.rem(me + k, n)
@@ -278,8 +288,46 @@
         left = jnp.concatenate([piece[0, b, at], piece[1, b, at]], axis=1)
         return [jnp.dot(left, wbuf[slot, i], preferred_element_type=F32) for i in range(2)]
 
+    per = rows // tok
+    blocks = rows // cols
+
+    def mix_place(k):
+        return k // per % 2, order(k // (2 * per)), (k % per) * tok
+
+    def build_mix(q):
+        b = order(q)
+
+        @pl.loop(0, G)
+        def _(m):
+            d_copy(b, m).wait_send()
+
+        if q == 0:
+            pl.when(z < L - 2)(f_copy(0).wait_send)
+            pl.when(z > 1)(f_copy(1).wait_send)
+        for k in range(2 * per * q, min(2 * per * (q + 1), blocks)):
+            c, b, first = mix_place(k)
+            lane = lax.broadcasted_iota(jnp.int32, (LANES, cols), 1) + k * cols
+            for r in range(nb):
+                value = jnp.zeros((LANES, cols), F32)
+                for e in range(k * cols // cap, ((k + 1) * cols - 1) // cap + 1):
+                    p = e * nb + r
+                    value = jnp.where(kcol[:, p : p + 1] == lane, wcol[:, p : p + 1], value)
+                piece[c, b, first + r * LANES : first + (r + 1) * LANES] = value.astype(BF16)
+
+    def ready_last():
+        @pl.loop(1, G)
+        def _(m):
+            @pl.when(jnp.logical_not(jnp.logical_and(m == far, next_to_end)))
+            def _():
+                e_copy(last, m).wait_recv()
+
+            d_copy(last, m).start()
+
     def finish(s):
         b, slot = order(s), s % 2
+
+        for q in range(L - 2):
+            pl.when(s == q + 1)(functools.partial(build_mix, q))
 
         @pl.loop(1, G)
         def _(j):
@@ -303,6 +351,7 @@
         @pl.loop(0, rows // tile)
         def _(t):
             at = pl.ds(pl.multiple_of(t * tile, 16), tile)
+            pl.when(jnp.logical_and(s == L - 2, t == rows // tile // 2))(ready_last)
             both = gate_up(b, slot, at)
 
             @pl.when(s == 0)
@@ -347,14 +396,14 @@
             return jnp.logical_and(z > 0, b == jnp.where(z > 1, z, L - 1))
         return jnp.logical_and(z < L - 1, b == jnp.where(z < L - 2, z, 0))
 
-    def add_extra(b):
+    def add_extra(b, held):
         for side in range(2):
             @pl.when(extra(b, side))
             def _():
                 a_copy(b, side).wait_recv()
-                tbuf[0:cap] += abuf[side].astype(F32)
-
-        obuf[b, far - 1] = tbuf[0:cap].astype(BF16)
+                held[0:cap] += abuf[side].astype(F32)
+
+        obuf[b, far - 1] = held[0:cap].astype(BF16)
 
     def project(i, m):
         b = order(L - 1 - i)
@@ -387,11 +436,14 @@
             @pl.when(jnp.logical_not(skipped(b)))
             def _():
                 e_copy(b, far).wait_send()
-                tbuf[0:cap] = result
 
                 @pl.when(i > 0)
                 def _():
-                    add_extra(b)
+                    tbuf[0:cap] = result
+
+                @pl.when(i == 0)
+                def _():
+                    ebuf[...] = result
 
     def each_send(i, act):
         b = order(L - 1 - i)
@@ -421,16 +473,7 @@
         def _(j):
             project(i, G - 1 - j)
 
-    last = order(L - 1)
-
-    @pl.loop(1, G)
-    def _(m):
-        @pl.when(jnp.logical_not(jnp.logical_and(m == far, next_to_end)))
-        def _():
-            e_copy(last, m).wait_recv()
-
-        d_copy(last, m).start()
-
+    build_mix(L - 2)
     for i in range(2):
         w_load(L - 1, i).wait()
     down_ready(last)
@@ -463,22 +506,11 @@
 
             @pl.when(jnp.logical_and(m == far, jnp.logical_not(jnp.logical_or(skipped(last), next_to_end))))
             def _():
-                obuf[last, far - 1] = tbuf[0:cap].astype(BF16)
+                obuf[last, far - 1] = ebuf[...].astype(BF16)
                 r_copy(last, far).start()
-
-    @pl.when(next_to_end)
-    def _():
-        add_extra(last)
-        r_copy(last, far).start()
-
-    project_all(1)
-    wait_sends(0)
-    start_sends(1)
 
     pl.when(z < L - 1)(z_copy(z, 0).wait_send)
     pl.when(z > 0)(z_copy(z, 1).wait_send)
-    pl.when(z < L - 2)(f_copy(0).wait_send)
-    pl.when(z > 1)(f_copy(1).wait_send)
     pl.when(next_to_end)(l_copy().wait_send)
 
     @pl.loop(0, L)
@@ -486,31 +518,9 @@
         pl.when(jnp.logical_and(b < z, z < L - 1))(z_copy(b, 0).wait_send)
         pl.when(jnp.logical_and(b > z, z > 0))(z_copy(b, 1).wait_send)
 
-        @pl.loop(0, G)
-        def _(m):
-            d_copy(b, m).wait_send()
-
         @pl.when(skipped(b))
         def _():
             rbuf[b, group_rows(flip(g, far, G))] = jnp.zeros((cap, cols), BF16)
-
-    per = rows // tok
-    blocks = rows // cols
-
-    def mix_place(k):
-        return k // (L * per), (k // per) % L, (k % per) * tok
-
-    for k in range(blocks):
-        c, b, first = mix_place(k)
-        lane = lax.broadcasted_iota(jnp.int32, (LANES, cols), 1) + k * cols
-        for r in range(nb):
-            value = jnp.zeros((LANES, cols), F32)
-            for e in range(k * cols // cap, ((k + 1) * cols - 1) // cap + 1):
-                q = e * nb + r
-                value = jnp.where(kcol[:, q : q + 1] == lane, wcol[:, q : q + 1], value)
-            piece[c, b, first + r * LANES : first + (r + 1) * LANES] = value.astype(BF16)
-
-    step = min(256, tok)
 
     def combined(b, t):
         parts = []
@@ -526,50 +536,59 @@
             def _():
                 r_copy(b, m).wait_recv()
 
-    @pl.loop(0, L - 1)
-    def _(i):
-        @pl.when(i > 0)
-        def _():
-            wait_sends(i)
-            start_sends(i + 1)
-
-        pl.when(i + 2 < L)(lambda: project_all(i + 2))
+    def combine(i):
         b = order(L - 1 - i)
         more = jnp.where(b > z, z, L - 1 - z) > 0
         arrived(b)
 
-        @pl.when(more)
-        def _():
-            remote(zbuf.at[b], rin.at[b], ys.at[b], yr.at[b], at_z(b)).wait_recv()
-
-        @pl.loop(0, tok // step)
+        @pl.loop(0, tiles)
         def _(t):
-            at = pl.ds(pl.multiple_of(t * step, 16), step)
+            at = rows_of(t)
             value = combined(b, t)
 
             @pl.when(more)
             def _():
+                y_wait(b, t)
                 zbuf[b, at] = (value + rin[b, at].astype(F32)).astype(BF16)
 
             @pl.when(jnp.logical_not(more))
             def _():
                 zbuf[b, at] = value.astype(BF16)
 
-        pl.when(b > z)(y_copy(b, 0).start)
-        pl.when(b < z)(y_copy(b, 1).start)
-
+            pl.when(b > z)(y_copy(b, 0, t).start)
+            pl.when(b < z)(y_copy(b, 1, t).start)
+
+    @pl.loop(1, L)
+    def _(i):
+        b = order(L - 1 - i)
+        project_all(i)
+        pl.when(jnp.logical_or(i > 1, jnp.logical_not(inside)))(lambda: wait_sends(i - 1))
+        pl.when(jnp.logical_not(skipped(b)))(lambda: add_extra(b, tbuf))
+        start_sends(i)
+
+        @pl.when(jnp.logical_and(next_to_end, i == 1))
+        def _():
+            add_extra(last, ebuf)
+            r_copy(last, far).start()
+
+        late = jnp.where(inside, 2, 1)
+        pl.when(i >= late)(lambda: combine(i - late))
+
+    pl.when(inside)(lambda: combine(L - 2))
     arrived(z)
 
-    @pl.loop(0, tok // step)
+    @pl.loop(0, tiles)
     def _(t):
-        at = pl.ds(pl.multiple_of(t * step, 16), step)
-        tbuf[at] = combined(z, t)
-
-    for side, slot in ((0, z), (1, L)):
-        @pl.when(z > 0 if side == 0 else z < L - 1)
-        def _():
-            remote(zbuf.at[z], rin.at[slot], ys.at[z], yr.at[slot], partner).wait_recv()
-            tbuf[...] += rin[slot].astype(F32)
+        tbuf[rows_of(t)] = combined(z, t)
+
+    @pl.loop(0, tiles)
+    def _(t):
+        at = rows_of(t)
+        for side, slot in ((0, z), (1, L)):
+            @pl.when(z > 0 if side == 0 else z < L - 1)
+            def _():
+                y_wait(slot, t)
+                tbuf[at] += rin[slot, at].astype(F32)
 
     stat2[me] = squares_of(tbuf[...], nb)
     for k in range(1, n):
@@ -594,13 +613,21 @@
         a_copy(z + 1, 0).wait_send()
         a_copy(z - 1, 1).wait_send()
 
+    pl.when(inside)(lambda: wait_sends(0))
     wait_sends(L - 1)
 
     @pl.loop(0, L)
     def _(b):
         down_push(b).wait_send()
-        pl.when(b > z)(y_copy(b, 0).wait_send)
-        pl.when(b < z)(y_copy(b, 1).wait_send)
+
+        @pl.loop(0, tiles)
+        def _(t):
+            pl.when(b > z)(y_copy(b, 0, t).wait_send)
+            pl.when(b < z)(y_copy(b, 1, t).wait_send)
+
+    @pl.loop(0, G)
+    def _(m):
+        d_copy(last, m).wait_send()
 
     @pl.loop(0, G)
     def _(m):
@@ -622,6 +649,7 @@
     units = gate_weight.shape[2]
     nb = tok // LANES
     tile = cap
+    tiles = tok // min(256, tok)
     vmem = pl.BlockSpec(memory_space=pltpu.VMEM)
     hbm = pl.BlockSpec(memory_space=pl.ANY)
     return pl.pallas_call(
@@ -641,6 +669,7 @@
             pltpu.VMEM((L, rows, cols), BF16),
             pltpu.VMEM((L + 1, tok, cols), BF16),
             pltpu.VMEM((2, cap, cols), BF16),
+            pltpu.VMEM((cap, cols), F32),
             pltpu.VMEM((tok, cols), F32),
             pltpu.VMEM((n, 2 * nb, LANES), F32),
             pltpu.VMEM((n, nb, LANES), F32),
@@ -657,7 +686,7 @@
             DMA((G,)), DMA((G,)),
             DMA((L, G)), DMA((L, G)),
             DMA((2,)), DMA((2,)),
-            DMA((L,)), DMA((L + 1,)),
+            DMA((L, tiles)), DMA((L + 1, tiles)),
             DMA((n,)), DMA((n,)),
             DMA((n,)), DMA((n,)),
             DMA((1,)),

time: 138 us -> 130 us (0.942)
  Pallas kernels: 136 us -> 128 us
    pallas_call x1, Pallas kernels: 136 us -> 128 us  [on_device(): pl.pallas_call(functools.partial(layer_kernel, L, G, cap, tile), out_shap...]
where the time goes in v3:
time: 130 us
  Pallas kernels  128 us (98%)
  local copies, waits for them, and re-layouts  1.87 us (1%)
    pallas_call x1, Pallas kernels, on_device(): pl.pallas_call(functools.partial(layer_kernel, L, G, cap, tile), out_shap...  128 us

profile of v3, /device:TPU:0, one launch (start us, length us, event | category | flops | bytes accessed | tf_op | source)
XLA Modules:
  0.0 129.6 jit_solution(7441111136997934631)
XLA Ops:
  0.0 127.7 %layer.1 = bf16[1024,256]{1,0:T(8,128)(2,1)} custom-call(bf16[1024,256]{1,0:T(8,128)(2,1)} %x_ref.1, bf16[256]{0:T(256)(128)(2,1)} %pre_ref.1, bf16[256]{0:T(256)(128)(2,1)} %post_ref.1, s32[2,1024]{1,0:T(2,128)} %bitcast.8, f32[2,1024]{1,0:T(2,128)} %bitcast.9, bf16[2048,896]{1,0:T(8,128)(2,1)} %bitcast.5, bf16[2048,896]{1,0:T(8,128)(2,1)} %bitcast.6, ...), custom_call_target="tpu_custom_call" | custom-call | tf_op jit(solution)/shard_map/layer/pallas_call | solution.py:655
  127.7 1.9 %copy.10 = bf16[1024,256]{1,0:T(8,128)(2,1)} copy(bf16[1024,256]{1,0:T(8,128)(2,1)} %layer.1) | data formatting | bytes 1048576

commit v4 on v3

--- a/solution.py
+++ b/solution.py
@@ -314,19 +314,10 @@
                     value = jnp.where(kcol[:, p : p + 1] == lane, wcol[:, p : p + 1], value)
                 piece[c, b, first + r * LANES : first + (r + 1) * LANES] = value.astype(BF16)
 
-    def ready_last():
-        @pl.loop(1, G)
-        def _(m):
-            @pl.when(jnp.logical_not(jnp.logical_and(m == far, next_to_end)))
-            def _():
-                e_copy(last, m).wait_recv()
-
-            d_copy(last, m).start()
-
     def finish(s):
         b, slot = order(s), s % 2
 
-        for q in range(L - 2):
+        for q in range(L - 3):
             pl.when(s == q + 1)(functools.partial(build_mix, q))
 
         @pl.loop(1, G)
@@ -351,7 +342,6 @@
         @pl.loop(0, rows // tile)
         def _(t):
             at = pl.ds(pl.multiple_of(t * tile, 16), tile)
-            pl.when(jnp.logical_and(s == L - 2, t == rows // tile // 2))(ready_last)
             both = gate_up(b, slot, at)
 
             @pl.when(s == 0)
@@ -389,7 +379,7 @@
             e_copy(farthest, far).wait_recv()
             l_copy().start()
 
-        finish(s - 1)
+        pl.when(s < L - 1)(lambda: finish(s - 1))
 
     def extra(b, side):
         if side == 0:
@@ -445,69 +435,131 @@
                 def _():
                     ebuf[...] = result
 
-    def each_send(i, act):
+    def sent(b, m):
+        return jnp.logical_not(jnp.logical_and(m == far, skipped(b)))
+
+    def wait_sends(i):
         b = order(L - 1 - i)
 
-        @pl.loop(0, G - 1)
+        @pl.loop(1, G)
+        def _(m):
+            pl.when(sent(b, m))(lambda: r_copy(b, m).wait_send())
+
+    def start_sends(i):
+        b = order(L - 1 - i)
+
+        @pl.loop(0, far)
         def _(j):
             m = far - j
-
-            @pl.when(jnp.logical_not(jnp.logical_and(m == far, skipped(b))))
-            def _():
-                act(b, m)
-
-    def start_sends(i):
-        each_send(i, lambda b, m: r_copy(b, m).start())
-
-    def wait_sends(i):
-        each_send(i, lambda b, m: r_copy(b, m).wait_send())
+            pl.when(sent(b, m))(lambda: r_copy(b, m).start())
 
     def down_ready(b):
         down_own(b).wait()
         down_push(b).wait_recv()
 
-    def project_all(i):
-        down_ready(order(L - 1 - i))
-
-        @pl.loop(0, G)
-        def _(j):
-            project(i, G - 1 - j)
+    before = second = order(L - 2)
+
+    def group_tiles(m, act):
+        first = flip(g, m, G) * cap
+
+        @pl.loop(0, cap // tile)
+        def _(t):
+            act(pl.ds(pl.multiple_of(first + t * tile, 16), tile))
+
+    def add_before(at):
+        both = gate_up(before, (L - 2) % 2, at)
+        for i in range(2):
+            acc[i, at] += both[i]
+
+    def hide(at):
+        both = gate_up(last, (L - 1) % 2, at)
+        both = [both[i] + acc[i, at] for i in range(2)]
+        half = 0.5 * both[0]
+        hbuf[core, at] = ((half + half * jnp.tanh(half)) * both[1]).astype(BF16)
+
+    def take_before(m):
+        d_copy(before, m).wait_recv()
+        group_tiles(m, add_before)
+
+    def close(m):
+        d_copy(last, m).wait_recv()
+        group_tiles(m, hide)
+        h_copy(m).start()
+
+    def send_first(m):
+        h_copy(m).wait_recv()
+        project(0, m)
+        r_copy(last, m).start()
+
+    build_mix(L - 3)
+
+    @pl.loop(1, G)
+    def _(m):
+        e_copy(before, m).wait_recv()
+        d_copy(before, m).start()
+
+    for s in (L - 2, L - 1):
+        for i in range(2):
+            w_load(s, i).wait()
+    down_ready(last)
+
+    @pl.loop(0, far)
+    def _(m):
+        take_before(m)
+        pl.when(m == 0)(lambda: close(0))
+
+        @pl.when(m == 1)
+        def _():
+            @pl.loop(1, far)
+            def _(k):
+                e_copy(last, k).wait_recv()
+                d_copy(last, k).start()
+
+    @pl.loop(1, G)
+    def _(m):
+        @pl.when(m == far)
+        def _():
+            @pl.when(jnp.logical_not(next_to_end))
+            def _():
+                e_copy(last, far).wait_recv()
+
+            d_copy(last, far).start()
+            send_first(far - 1)
+            take_before(far)
+
+        close(m)
+        pl.when(jnp.logical_and(m > 1, m < far))(lambda: send_first(m - 1))
+
+    down_ready(second)
+
+    @pl.loop(1, far)
+    def _(m):
+        project(1, m)
+
+    h_copy(far).wait_recv()
+
+    @pl.loop(0, 2)
+    def _(i):
+        project(1 - i, far)
+
+        @pl.when(i == 0)
+        def _():
+            pl.when(sent(second, far))(lambda: add_extra(second, tbuf))
+            pl.when(jnp.logical_not(inside))(lambda: wait_sends(0))
+            start_sends(1)
+
+    h_copy(0).wait_recv()
+
+    @pl.loop(0, 2)
+    def _(i):
+        project(i, 0)
+
+    @pl.when(jnp.logical_not(jnp.logical_or(skipped(last), next_to_end)))
+    def _():
+        obuf[last, far - 1] = ebuf[...].astype(BF16)
+        r_copy(last, far).start()
 
     build_mix(L - 2)
-    for i in range(2):
-        w_load(L - 1, i).wait()
-    down_ready(last)
-
-    @pl.loop(0, G + 1)
-    def _(q):
-        @pl.when(q < G)
-        def _():
-            m = lax.rem(q + 1, G)
-            d_copy(last, m).wait_recv()
-            first = flip(g, m, G) * cap
-
-            @pl.loop(0, cap // tile)
-            def _(t):
-                at = pl.ds(pl.multiple_of(first + t * tile, 16), tile)
-                both = gate_up(last, (L - 1) % 2, at)
-                gates = acc[0, at] + both[0]
-                half = 0.5 * gates
-                hbuf[core, at] = ((half + half * jnp.tanh(half)) * (acc[1, at] + both[1])).astype(BF16)
-
-            h_copy(m).start()
-
-        @pl.when(q > 0)
-        def _():
-            m = lax.rem(q, G)
-            h_copy(m).wait_recv()
-            project(0, m)
-            direct = jnp.logical_and(m > 0, m < far)
-            pl.when(direct)(lambda: r_copy(last, m).start())
-
-            @pl.when(jnp.logical_and(m == far, jnp.logical_not(jnp.logical_or(skipped(last), next_to_end))))
-            def _():
-                obuf[last, far - 1] = ebuf[...].astype(BF16)
-                r_copy(last, far).start()
 
     pl.when(z < L - 1)(z_copy(z, 0).wait_send)
     pl.when(z > 0)(z_copy(z, 1).wait_send)
@@ -561,15 +613,27 @@
     @pl.loop(1, L)
     def _(i):
         b = order(L - 1 - i)
-        project_all(i)
-        pl.when(jnp.logical_or(i > 1, jnp.logical_not(inside)))(lambda: wait_sends(i - 1))
-        pl.when(jnp.logical_not(skipped(b)))(lambda: add_extra(b, tbuf))
-        start_sends(i)
-
-        @pl.when(jnp.logical_and(next_to_end, i == 1))
-        def _():
-            add_extra(last, ebuf)
-            r_copy(last, far).start()
+
+        @pl.when(i > 1)
+        def _():
+            down_ready(b)
+
+            @pl.loop(0, far)
+            def _(j):
+                project(i, far - j)
+
+            @pl.when(jnp.logical_and(next_to_end, i == 2))
+            def _():
+                add_extra(last, ebuf)
+                r_copy(last, far).start()
+
+            pl.when(sent(b, far))(lambda: add_extra(b, tbuf))
+
+            wait_sends(i - 1)
+
+            start_sends(i)
+
+            project(i, 0)
 
         late = jnp.where(inside, 2, 1)
         pl.when(i >= late)(lambda: combine(i - late))
@@ -589,6 +653,10 @@
             def _():
                 y_wait(slot, t)
                 tbuf[at] += rin[slot, at].astype(F32)
+
+    def out_copy(t):
+        at = slice(t * step, (t + 1) * step)
+        return pltpu.make_async_copy(nbuf.at[at], out_ref.at[at], xs.at[t])
 
     stat2[me] = squares_of(tbuf[...], nb)
     for k in range(1, n):
@@ -598,8 +666,8 @@
     for r in range(nb):
         at = slice(r * LANES, (r + 1) * LANES)
         nbuf[at] = (tbuf[at] * scol[:, r : r + 1] * post).astype(BF16)
-    out_copy = pltpu.make_async_copy(nbuf, out_ref, xs.at[0])
-    out_copy.start()
+        if (r + 1) * LANES % step == 0:
+            out_copy(r * LANES // step).start()
 
     for k in range(1, n):
         stat_copy(stat, ss, sr, k).wait_send()
@@ -633,7 +701,8 @@
     def _(m):
         h_copy(m).wait_send()
 
-    out_copy.wait()
+    for t in range(tiles):
+        out_copy(t).wait()
 
 
 def on_device(
@@ -689,7 +758,7 @@
             DMA((L, tiles)), DMA((L + 1, tiles)),
             DMA((n,)), DMA((n,)),
             DMA((n,)), DMA((n,)),
-            DMA((1,)),
+            DMA((tiles,)),
         ],
         compiler_params=pltpu.CompilerParams(
             collective_id=1, has_side_effects=True, vmem_limit_bytes=62 * 2**20

time: 130 us -> 126 us (0.969)
  Pallas kernels: 128 us -> 124 us
    pallas_call x1, Pallas kernels: 128 us -> 124 us  [on_device(): pl.pallas_call(functools.partial(layer_kernel, L, G, cap, tile), out_shap...]
where the time goes in v4:
time: 126 us; the launch traced here: 125 us
  Pallas kernels  124 us (98%)
  local copies, waits for them, and re-layouts  1.87 us (1%)
    pallas_call x1, Pallas kernels, on_device(): pl.pallas_call(functools.partial(layer_kernel, L, G, cap, tile), out_shap...  124 us

profile of v4, /device:TPU:0, one launch (start us, length us, event | category | flops | bytes accessed | tf_op | source)
XLA Modules:
  0.0 125.5 jit_solution(1074299027586650862)
XLA Ops:
  0.0 123.6 %layer.1 = bf16[1024,256]{1,0:T(8,128)(2,1)} custom-call(bf16[1024,256]{1,0:T(8,128)(2,1)} %x_ref.1, bf16[256]{0:T(256)(128)(2,1)} %pre_ref.1, bf16[256]{0:T(256)(128)(2,1)} %post_ref.1, s32[2,1024]{1,0:T(2,128)} %bitcast.8, f32[2,1024]{1,0:T(2,128)} %bitcast.9, bf16[2048,896]{1,0:T(8,128)(2,1)} %bitcast.5, bf16[2048,896]{1,0:T(8,128)(2,1)} %bitcast.6, ...), custom_call_target="tpu_custom_call" | custom-call | tf_op jit(solution)/shard_map/layer/pallas_call | solution.py:724
  123.6 1.9 %copy.10 = bf16[1024,256]{1,0:T(8,128)(2,1)} copy(bf16[1024,256]{1,0:T(8,128)(2,1)} %layer.1) | data formatting | bytes 1048576

commit v5 on v4

--- a/solution.py
+++ b/solution.py
@@ -139,9 +139,16 @@
         area = piece.at[core, b, group_rows(flip(g, m, G))]
         return remote(area, area, ds.at[b, m], dr.at[b, m], partner)
 
-    def h_copy(m):
-        area = hbuf.at[core, group_rows(flip(g, m, G))]
-        return remote(area, area, hs.at[m], hr.at[m], partner)
+    half = cap // 2 if cap % 32 == 0 else cap
+
+    def h_copy(m, t):
+        at = pl.ds(pl.multiple_of(flip(g, m, G) * cap + t * half, 16), half)
+        area = hbuf.at[core, at]
+        return remote(area, area, hs.at[m, t], hr.at[m, t], partner)
+
+    def h_wait(m):
+        for t in range(cap // half):
+            h_copy(m, t).wait_recv()
 
     def r_copy(b, m):
         return remote(
@@ -359,27 +366,24 @@
             for i in range(2):
                 w_load(s + 2, i).start()
 
-    process(0)
-
-    @pl.loop(1, L)
+    @pl.loop(0, L)
     def _(s):
-        @pl.when(jnp.logical_or(jnp.logical_not(inside), s == 1))
-        def _():
-            take(s)
-            pl.when(inside)(lambda: take(s + 1))
-            process(s)
-
-        @pl.when(jnp.logical_and(inside, s + 1 < L))
-        def _():
-            pl.when(s > 1)(lambda: take(s + 1))
-            process(s + 1)
+        early = jnp.logical_and(inside, s > 0)
+        low = jnp.where(jnp.logical_and(early, s > 1), s + 1, s)
+        high = jnp.where(early, jnp.minimum(s + 2, L), s + 1)
+
+        @pl.when(s > 0)
+        def _():
+            pl.loop(low, high)(take)
+
+        pl.loop(low, high)(process)
 
         @pl.when(jnp.logical_and(next_to_end, s == L - 1))
         def _():
             e_copy(farthest, far).wait_recv()
             l_copy().start()
 
-        pl.when(s < L - 1)(lambda: finish(s - 1))
+        pl.when(jnp.logical_and(s > 0, s < L - 1))(lambda: finish(s - 1))
 
     def extra(b, side):
         if side == 0:
@@ -445,9 +449,7 @@
         def _(m):
             pl.when(sent(b, m))(lambda: r_copy(b, m).wait_send())
 
-    def start_sends(i):
-        b = order(L - 1 - i)
-
+    def start_sends(b):
         @pl.loop(0, far)
         def _(j):
             m = far - j
@@ -459,37 +461,23 @@
 
     before = second = order(L - 2)
 
-    def group_tiles(m, act):
-        first = flip(g, m, G) * cap
-
-        @pl.loop(0, cap // tile)
-        def _(t):
-            act(pl.ds(pl.multiple_of(first + t * tile, 16), tile))
-
-    def add_before(at):
+    def take_before(m):
+        d_copy(before, m).wait_recv()
+        at = group_rows(flip(g, m, G))
         both = gate_up(before, (L - 2) % 2, at)
         for i in range(2):
             acc[i, at] += both[i]
 
-    def hide(at):
-        both = gate_up(last, (L - 1) % 2, at)
-        both = [both[i] + acc[i, at] for i in range(2)]
-        half = 0.5 * both[0]
-        hbuf[core, at] = ((half + half * jnp.tanh(half)) * both[1]).astype(BF16)
-
-    def take_before(m):
-        d_copy(before, m).wait_recv()
-        group_tiles(m, add_before)
-
     def close(m):
         d_copy(last, m).wait_recv()
-        group_tiles(m, hide)
-        h_copy(m).start()
-
-    def send_first(m):
-        h_copy(m).wait_recv()
-        project(0, m)
-        r_copy(last, m).start()
+
+        @pl.loop(0, cap // half)
+        def _(t):
+            at = pl.ds(pl.multiple_of(flip(g, m, G) * cap + t * half, 16), half)
+            both = gate_up(last, (L - 1) % 2, at)
+            gates = 0.5 * (both[0] + acc[0, at])
+            hbuf[core, at] = ((gates + gates * jnp.tanh(gates)) * (both[1] + acc[1, at])).astype(BF16)
+            h_copy(m, t).start()
 
     build_mix(L - 3)
 
@@ -502,77 +490,56 @@
         for i in range(2):
             w_load(s, i).wait()
     down_ready(last)
-
-    @pl.loop(0, far)
-    def _(m):
-        take_before(m)
-        pl.when(m == 0)(lambda: close(0))
-
-        @pl.when(m == 1)
+    down_ready(second)
+
+    @pl.loop(0, 2 * far + 1)
+    def _(v):
+        u = v - far
+        pl.when(jnp.logical_or(v < far, u == far))(lambda: take_before(jnp.minimum(v, far)))
+
+        @pl.when(v == 1)
         def _():
             @pl.loop(1, far)
             def _(k):
                 e_copy(last, k).wait_recv()
                 d_copy(last, k).start()
 
-    @pl.loop(1, G)
-    def _(m):
-        @pl.when(m == far)
+        @pl.when(u == far - 1)
         def _():
             @pl.when(jnp.logical_not(next_to_end))
             def _():
                 e_copy(last, far).wait_recv()
 
             d_copy(last, far).start()
-            send_first(far - 1)
-            take_before(far)
-
-        close(m)
-        pl.when(jnp.logical_and(m > 1, m < far))(lambda: send_first(m - 1))
-
-    down_ready(second)
-
-    @pl.loop(1, far)
-    def _(m):
-        project(1, m)
-
-    h_copy(far).wait_recv()
-
-    @pl.loop(0, 2)
-    def _(i):
-        project(1 - i, far)
-
-        @pl.when(i == 0)
-        def _():
-            pl.when(sent(second, far))(lambda: add_extra(second, tbuf))
-            pl.when(jnp.logical_not(inside))(lambda: wait_sends(0))
-            start_sends(1)
-
-    h_copy(0).wait_recv()
-
-    @pl.loop(0, 2)
-    def _(i):
-        project(i, 0)
-
-    @pl.when(jnp.logical_not(jnp.logical_or(skipped(last), next_to_end)))
-    def _():
+
+        @pl.when(jnp.logical_or(v == 0, jnp.logical_and(u >= 0, u != far - 1)))
+        def _():
+            close(jnp.where(v == 0, 0, jnp.minimum(u + 1, far)))
+
+        @pl.when(jnp.logical_and(u > 0, u < far))
+        def _():
+            h_wait(u)
+            project(0, u)
+            r_copy(last, u).start()
+
+    def first_far():
         obuf[last, far - 1] = ebuf[...].astype(BF16)
         r_copy(last, far).start()
 
-    build_mix(L - 2)
-
-    pl.when(z < L - 1)(z_copy(z, 0).wait_send)
-    pl.when(z > 0)(z_copy(z, 1).wait_send)
-    pl.when(next_to_end)(l_copy().wait_send)
-
-    @pl.loop(0, L)
-    def _(b):
-        pl.when(jnp.logical_and(b < z, z < L - 1))(z_copy(b, 0).wait_send)
-        pl.when(jnp.logical_and(b > z, z > 0))(z_copy(b, 1).wait_send)
-
-        @pl.when(skipped(b))
-        def _():
-            rbuf[b, group_rows(flip(g, far, G))] = jnp.zeros((cap, cols), BF16)
+    def after_dispatch():
+        build_mix(L - 2)
+        pl.when(z < L - 1)(z_copy(z, 0).wait_send)
+        pl.when(z > 0)(z_copy(z, 1).wait_send)
+        pl.when(next_to_end)(l_copy().wait_send)
+
+        @pl.loop(0, L)
+        def _(b):
+            pl.when(jnp.logical_and(b < z, z < L - 1))(z_copy(b, 0).wait_send)
+            pl.when(jnp.logical_and(b > z, z > 0))(z_copy(b, 1).wait_send)
+
+            @pl.when(skipped(b))
+            def _():
+                rbuf[b, group_rows(flip(g, far, G))] = jnp.zeros((cap, cols), BF16)
 
     def combined(b, t):
         parts = []
@@ -590,7 +557,9 @@
 
     def combine(i):
         b = order(L - 1 - i)
-        more = jnp.where(b > z, z, L - 1 - z) > 0
+        own = b == z
+        more = jnp.logical_and(jnp.logical_not(own), jnp.where(b > z, z, L - 1 - z) > 0)
+        ends_here = jnp.logical_or(own, more)
         arrived(b)
 
         @pl.loop(0, tiles)
@@ -598,52 +567,60 @@
             at = rows_of(t)
             value = combined(b, t)
 
+            @pl.when(own)
+            def _():
+                tbuf[at] = value
+
             @pl.when(more)
             def _():
                 y_wait(b, t)
                 zbuf[b, at] = (value + rin[b, at].astype(F32)).astype(BF16)
 
-            @pl.when(jnp.logical_not(more))
+            @pl.when(jnp.logical_not(ends_here))
             def _():
                 zbuf[b, at] = value.astype(BF16)
 
             pl.when(b > z)(y_copy(b, 0, t).start)
             pl.when(b < z)(y_copy(b, 1, t).start)
 
-    @pl.loop(1, L)
+    def launch(i):
+        b = order(L - 1 - i)
+
+        @pl.when(jnp.logical_and(next_to_end, i == 2))
+        def _():
+            add_extra(last, ebuf)
+            r_copy(last, far).start()
+
+        pl.when(sent(b, far))(lambda: add_extra(b, tbuf))
+        pl.when(jnp.logical_or(i > 1, jnp.logical_not(inside)))(lambda: wait_sends(i - 1))
+        start_sends(b)
+
+    late = jnp.where(inside, 2, 1)
+
+    @pl.loop(1, L + 2)
     def _(i):
-        b = order(L - 1 - i)
-
-        @pl.when(i > 1)
-        def _():
-            down_ready(b)
-
-            @pl.loop(0, far)
+        first = i == 1
+
+        @pl.when(i < L)
+        def _():
+            pl.when(i > 1)(lambda: down_ready(order(L - 1 - i)))
+
+            @pl.loop(0, jnp.where(first, G + 2, G))
             def _(j):
-                project(i, far - j)
-
-            @pl.when(jnp.logical_and(next_to_end, i == 2))
-            def _():
-                add_extra(last, ebuf)
-                r_copy(last, far).start()
-
-            pl.when(sent(b, far))(lambda: add_extra(b, tbuf))
-
-            wait_sends(i - 1)
-
-            start_sends(i)
-
-            project(i, 0)
-
-        late = jnp.where(inside, 2, 1)
-        pl.when(i >= late)(lambda: combine(i - late))
-
-    pl.when(inside)(lambda: combine(L - 2))
-    arrived(z)
-
-    @pl.loop(0, tiles)
-    def _(t):
-        tbuf[rows_of(t)] = combined(z, t)
+                pl.when(jnp.logical_and(first, j == far - 1))(lambda: h_wait(far))
+                pl.when(jnp.logical_and(first, j == far + 1))(lambda: h_wait(0))
+                m = jnp.where(first, jnp.where(j < far, j + 1, jnp.where(j == far, far, 0)), far - j)
+                rest = jnp.logical_and(first, jnp.logical_or(j == far, j == far + 1))
+                project(jnp.where(rest, 0, i), m)
+                pl.when(j == far - 1)(lambda: launch(i))
+
+        @pl.when(first)
+        def _():
+            pl.when(jnp.logical_not(jnp.logical_or(skipped(last), next_to_end)))(first_far)
+            after_dispatch()
+
+        c = i - late
+        pl.when(jnp.logical_and(c >= 0, c < L))(lambda: combine(c))
 
     @pl.loop(0, tiles)
     def _(t):
@@ -661,6 +638,38 @@
     stat2[me] = squares_of(tbuf[...], nb)
     for k in range(1, n):
         stat_copy(stat2, ts, tr, k).start()
+    for k in range(1, n):
+        stat_copy(stat, ss, sr, k).wait_send()
+
+    pl.when(z == 0)(a_copy(farthest, 0).wait_send)
+    pl.when(z == L - 1)(a_copy(farthest, 1).wait_send)
+
+    @pl.when(inside)
+    def _():
+        a_copy(z + 1, 0).wait_send()
+        a_copy(z - 1, 1).wait_send()
+
+    pl.when(inside)(lambda: wait_sends(0))
+    wait_sends(L - 1)
+
+    @pl.loop(0, L)
+    def _(b):
+        down_push(b).wait_send()
+
+        @pl.loop(0, tiles)
+        def _(t):
+            pl.when(b > z)(y_copy(b, 0, t).wait_send)
+            pl.when(b < z)(y_copy(b, 1, t).wait_send)
+
+    @pl.loop(0, G)
+    def _(m):
+        d_copy(last, m).wait_send()
+
+    @pl.loop(0, G)
+    def _(m):
+        for t in range(cap // half):
+            h_copy(m, t).wait_send()
+
     post = post_ref[...].astype(F32).reshape(1, cols)
     scol[...] = row_scale(stat2, ts, tr)
     for r in range(nb):
@@ -670,37 +679,7 @@
             out_copy(r * LANES // step).start()
 
     for k in range(1, n):
-        stat_copy(stat, ss, sr, k).wait_send()
         stat_copy(stat2, ts, tr, k).wait_send()
-
-    pl.when(z == 0)(a_copy(farthest, 0).wait_send)
-    pl.when(z == L - 1)(a_copy(farthest, 1).wait_send)
-
-    @pl.when(inside)
-    def _():
-        a_copy(z + 1, 0).wait_send()
-        a_copy(z - 1, 1).wait_send()
-
-    pl.when(inside)(lambda: wait_sends(0))
-    wait_sends(L - 1)
-
-    @pl.loop(0, L)
-    def _(b):
-        down_push(b).wait_send()
-
-        @pl.loop(0, tiles)
-        def _(t):
-            pl.when(b > z)(y_copy(b, 0, t).wait_send)
-            pl.when(b < z)(y_copy(b, 1, t).wait_send)
-
-    @pl.loop(0, G)
-    def _(m):
-        d_copy(last, m).wait_send()
-
-    @pl.loop(0, G)
-    def _(m):
-        h_copy(m).wait_send()
-
     for t in range(tiles):
         out_copy(t).wait()
 
@@ -752,7 +731,7 @@
             DMA((L, G)), DMA((L, G)),
             DMA((2, 2)),
             DMA((L,)), DMA((L,)), DMA((L,)),
-            DMA((G,)), DMA((G,)),
+            DMA((G, 2)), DMA((G, 2)),
             DMA((L, G)), DMA((L, G)),
             DMA((2,)), DMA((2,)),
             DMA((L, tiles)), DMA((L + 1, tiles)),

time: 126 us -> 125 us (level)
  no operation moved by 1% of the time
where the time goes in v5:
time: 125 us
  Pallas kernels  123 us (98%)
  local copies, waits for them, and re-layouts  1.87 us (1%)
    pallas_call x1, Pallas kernels, on_device(): pl.pallas_call(functools.partial(layer_kernel, L, G, cap, tile), out_shap...  123 us

profile of v5, /device:TPU:0, one launch (start us, length us, event | category | flops | bytes accessed | tf_op | source)
XLA Modules:
  0.0 124.6 jit_solution(16994085595204977195)
XLA Ops:
  0.0 122.7 %layer.1 = bf16[1024,256]{1,0:T(8,128)(2,1)} custom-call(bf16[1024,256]{1,0:T(8,128)(2,1)} %x_ref.1, bf16[256]{0:T(256)(128)(2,1)} %pre_ref.1, bf16[256]{0:T(256)(128)(2,1)} %post_ref.1, s32[2,1024]{1,0:T(2,128)} %bitcast.8, f32[2,1024]{1,0:T(2,128)} %bitcast.9, bf16[2048,896]{1,0:T(8,128)(2,1)} %bitcast.5, bf16[2048,896]{1,0:T(8,128)(2,1)} %bitcast.6, ...), custom_call_target="tpu_custom_call" | custom-call | tf_op jit(solution)/shard_map/layer/pallas_call | solution.py:703
  122.7 1.9 %copy.10 = bf16[1024,256]{1,0:T(8,128)(2,1)} copy(bf16[1024,256]{1,0:T(8,128)(2,1)} %layer.1) | data formatting | bytes 1048576

commit v6 on v5

--- a/solution.py
+++ b/solution.py
@@ -55,7 +55,7 @@
     x_ref, pre_ref, post_ref, ids_ref, rw_ref, gate_ref, up_ref, down_ref, out_ref,
     zbuf, nbuf, obuf, piece, wbuf, acc, hbuf, dbuf, rbuf, rin, abuf, ebuf, tbuf,
     stat, stat2, kbuf, kcol, wcol, scol,
-    zs, zr, es, er, fs, ds, dr, ws, dl, dps, dpr, hs, hr, rs, rr, as_, ar, ys, yr, ss, sr, ts, tr, xs,
+    zs, zr, es, er, fs, ds, dr, ws, dl, dps, dpr, hs, hr, rr, as_, ar, ys, yr, ss, sr, ts, tr, xs,
 ):
     tok, cols = nbuf.shape
     nb = tok // LANES
@@ -112,12 +112,16 @@
         return down_ref.at[:, pl.ds(pl.multiple_of((b * 2 + c) * cols, LANES), cols)]
 
     def down_own(b):
-        return pltpu.make_async_copy(down_part(b, core), dbuf.at[b, my_units(core)], dl.at[b])
+        return pltpu.make_async_copy(down_part(b, core), dbuf.at[b, my_units(core)], dl.at[0])
 
     def down_push(b):
         return remote(
-            down_part(b, 1 - core), dbuf.at[b, my_units(core)], dps.at[b], dpr.at[b], partner
+            down_part(b, 1 - core), dbuf.at[b, my_units(core)], dps.at[0], dpr.at[0], partner
         )
+
+    def down_all(send, recv):
+        area = dbuf.at[:, my_units(core)]
+        return remote(area, area, send.at[0], recv.at[0], partner)
 
     def z_copy(b, side):
         return remote(zbuf.at[b], zbuf.at[b], zs.at[side, b], zr.at[b], at_z(z + 1 - 2 * side))
@@ -137,22 +141,29 @@
 
     def d_copy(b, m):
         area = piece.at[core, b, group_rows(flip(g, m, G))]
-        return remote(area, area, ds.at[b, m], dr.at[b, m], partner)
+        return remote(area, area, ds.at[b], dr.at[b, m], partner)
 
     half = cap // 2 if cap % 32 == 0 else cap
+
+    def d_sent(b):
+        area = piece.at[core, b]
+        remote(area, area, ds.at[b], dr.at[b, 0], partner).wait_send()
 
     def h_copy(m, t):
         at = pl.ds(pl.multiple_of(flip(g, m, G) * cap + t * half, 16), half)
         area = hbuf.at[core, at]
-        return remote(area, area, hs.at[m, t], hr.at[m, t], partner)
+        return remote(area, area, hs.at[m], hr.at[m], partner)
+
+    def h_all(m):
+        area = hbuf.at[core, group_rows(flip(g, m, G))]
+        return remote(area, area, hs.at[m], hr.at[m], partner)
 
     def h_wait(m):
-        for t in range(cap // half):
-            h_copy(m, t).wait_recv()
+        h_all(m).wait_recv()
 
     def r_copy(b, m):
         return remote(
-            obuf.at[b, m - 1], rbuf.at[b, group_rows(g)], rs.at[b, m], rr.at[b, m], at_g(m)
+            obuf.at[b, m - 1], rbuf.at[b, group_rows(g)], es.at[b, m], rr.at[b, m], at_g(m)
         )
 
     def a_copy(b, side):
@@ -164,19 +175,19 @@
     def y_copy(b, side, t):
         to = z + 1 - 2 * side
         slot = jnp.where(jnp.logical_and(to == b, side == 1), L, b)
-        return remote(zbuf.at[b, rows_of(t)], rin.at[slot, rows_of(t)], ys.at[b, t], yr.at[slot, t], at_z(to))
+        return remote(zbuf.at[b, rows_of(t)], rin.at[slot, rows_of(t)], ys.at[b], yr.at[slot, t], at_z(to))
 
     def y_wait(slot, t):
         area = rin.at[slot, rows_of(t)]
-        remote(area, area, ys.at[0, t], yr.at[slot, t], partner).wait_recv()
+        remote(area, area, ys.at[0], yr.at[slot, t], partner).wait_recv()
 
     def stat_copy(buf, send, recv, k):
         to = lax.rem(me + k, n)
-        return remote(buf.at[me], buf.at[me], send.at[to], recv.at[me], {"tp": to})
-
-    def stat_wait(buf, send, recv, k):
-        of = lax.rem(me + n - k, n)
-        remote(buf.at[of], buf.at[of], send.at[of], recv.at[of], {"tp": of}).wait_recv()
+        return remote(buf.at[me], buf.at[me], send.at[0], recv.at[0], {"tp": to})
+
+    def stat_all(buf, send, recv):
+        area = buf.at[0 : n - 1]
+        return remote(area, area, send.at[0], recv.at[0], partner)
 
     barrier = pltpu.get_barrier_semaphore()
     for k in range(1, n):
@@ -243,8 +254,7 @@
             ).astype(BF16)
 
     def row_scale(buf, send, recv):
-        for k in range(1, n):
-            stat_wait(buf, send, recv, k)
+        stat_all(buf, send, recv).wait_recv()
         total = buf[0, 0:nb]
         for k in range(1, n):
             total = total + buf[k, 0:nb]
@@ -304,10 +314,7 @@
     def build_mix(q):
         b = order(q)
 
-        @pl.loop(0, G)
-        def _(m):
-            d_copy(b, m).wait_send()
-
+        d_sent(b)
         if q == 0:
             pl.when(z < L - 2)(f_copy(0).wait_send)
             pl.when(z > 1)(f_copy(1).wait_send)
@@ -455,9 +462,9 @@
             m = far - j
             pl.when(sent(b, m))(lambda: r_copy(b, m).start())
 
-    def down_ready(b):
-        down_own(b).wait()
-        down_push(b).wait_recv()
+    def down_ready():
+        down_all(dps, dl).wait_recv()
+        down_all(dps, dpr).wait_recv()
 
     before = second = order(L - 2)
 
@@ -489,8 +496,7 @@
     for s in (L - 2, L - 1):
         for i in range(2):
             w_load(s, i).wait()
-    down_ready(last)
-    down_ready(second)
+    down_ready()
 
     @pl.loop(0, 2 * far + 1)
     def _(v):
@@ -603,8 +609,6 @@
 
         @pl.when(i < L)
         def _():
-            pl.when(i > 1)(lambda: down_ready(order(L - 1 - i)))
-
             @pl.loop(0, jnp.where(first, G + 2, G))
             def _(j):
                 pl.when(jnp.logical_and(first, j == far - 1))(lambda: h_wait(far))
@@ -632,14 +636,13 @@
                 tbuf[at] += rin[slot, at].astype(F32)
 
     def out_copy(t):
-        at = slice(t * step, (t + 1) * step)
-        return pltpu.make_async_copy(nbuf.at[at], out_ref.at[at], xs.at[t])
+        at = slice(t * LANES, (t + 1) * LANES)
+        return pltpu.make_async_copy(nbuf.at[at], out_ref.at[at], xs.at[0])
 
     stat2[me] = squares_of(tbuf[...], nb)
     for k in range(1, n):
         stat_copy(stat2, ts, tr, k).start()
-    for k in range(1, n):
-        stat_copy(stat, ss, sr, k).wait_send()
+    stat_all(stat, ss, sr).wait_send()
 
     pl.when(z == 0)(a_copy(farthest, 0).wait_send)
     pl.when(z == L - 1)(a_copy(farthest, 1).wait_send)
@@ -652,36 +655,29 @@
     pl.when(inside)(lambda: wait_sends(0))
     wait_sends(L - 1)
 
+    down_all(dps, dpr).wait_send()
+
     @pl.loop(0, L)
     def _(b):
-        down_push(b).wait_send()
-
-        @pl.loop(0, tiles)
-        def _(t):
-            pl.when(b > z)(y_copy(b, 0, t).wait_send)
-            pl.when(b < z)(y_copy(b, 1, t).wait_send)
+        @pl.when(b != z)
+        def _():
+            remote(zbuf.at[b], zbuf.at[b], ys.at[b], zr.at[b], partner).wait_send()
+
+    d_sent(last)
 
     @pl.loop(0, G)
     def _(m):
-        d_copy(last, m).wait_send()
-
-    @pl.loop(0, G)
-    def _(m):
-        for t in range(cap // half):
-            h_copy(m, t).wait_send()
-
-    post = post_ref[...].astype(F32).reshape(1, cols)
-    scol[...] = row_scale(stat2, ts, tr)
+        h_all(m).wait_send()
+
+    tbuf[...] = tbuf[...] * post_ref[...].astype(F32).reshape(1, cols)
+    scale = row_scale(stat2, ts, tr)
     for r in range(nb):
         at = slice(r * LANES, (r + 1) * LANES)
-        nbuf[at] = (tbuf[at] * scol[:, r : r + 1] * post).astype(BF16)
-        if (r + 1) * LANES % step == 0:
-            out_copy(r * LANES // step).start()
-
-    for k in range(1, n):
-        stat_copy(stat2, ts, tr, k).wait_send()
-    for t in range(tiles):
-        out_copy(t).wait()
+        nbuf[at] = (tbuf[at] * scale[:, r : r + 1]).astype(BF16)
+        out_copy(r).start()
+
+    stat_all(stat2, ts, tr).wait_send()
+    pltpu.make_async_copy(nbuf, out_ref, xs.at[0]).wait()
 
 
 def on_device(
@@ -728,16 +724,16 @@
             DMA((2, L)), DMA((L,)),
             DMA((L, G)), DMA((L, G)),
             DMA((3,)),
-            DMA((L, G)), DMA((L, G)),
+            DMA((L,)), DMA((L, G)),
             DMA((2, 2)),
-            DMA((L,)), DMA((L,)), DMA((L,)),
-            DMA((G, 2)), DMA((G, 2)),
-            DMA((L, G)), DMA((L, G)),
+            DMA((1,)), DMA((1,)), DMA((1,)),
+            DMA((G,)), DMA((G,)),
+            DMA((L, G)),
             DMA((2,)), DMA((2,)),
-            DMA((L, tiles)), DMA((L + 1, tiles)),
-            DMA((n,)), DMA((n,)),
-            DMA((n,)), DMA((n,)),
-            DMA((tiles,)),
+            DMA((L,)), DMA((L + 1, tiles)),
+            DMA((1,)), DMA((1,)),
+            DMA((1,)), DMA((1,)),
+            DMA((1,)),
         ],
         compiler_params=pltpu.CompilerParams(
             collective_id=1, has_side_effects=True, vmem_limit_bytes=62 * 2**20

time: 125 us -> 124 us (level)
  no operation moved by 1% of the time
where the time goes in v6:
time: 124 us
  Pallas kernels  122 us (98%)
  local copies, waits for them, and re-layouts  1.87 us (2%)
    pallas_call x1, Pallas kernels, on_device(): pl.pallas_call(functools.partial(layer_kernel, L, G, cap, tile), out_shap...  122 us

profile of v6, /device:TPU:0, one launch (start us, length us, event | category | flops | bytes accessed | tf_op | source)
XLA Modules:
  0.0 123.8 jit_solution(12006345405206291726)
XLA Ops:
  0.0 121.9 %layer.1 = bf16[1024,256]{1,0:T(8,128)(2,1)} custom-call(bf16[1024,256]{1,0:T(8,128)(2,1)} %x_ref.1, bf16[256]{0:T(256)(128)(2,1)} %pre_ref.1, bf16[256]{0:T(256)(128)(2,1)} %post_ref.1, s32[2,1024]{1,0:T(2,128)} %bitcast.8, f32[2,1024]{1,0:T(2,128)} %bitcast.9, bf16[2048,896]{1,0:T(8,128)(2,1)} %bitcast.5, bf16[2048,896]{1,0:T(8,128)(2,1)} %bitcast.6, ...), custom_call_target="tpu_custom_call" | custom-call | tf_op jit(solution)/shard_map/layer/pallas_call | solution.py:699
  121.9 1.9 %copy.10 = bf16[1024,256]{1,0:T(8,128)(2,1)} copy(bf16[1024,256]{1,0:T(8,128)(2,1)} %layer.1) | data formatting | bytes 1048576

commit v7 on v6

--- a/solution.py
+++ b/solution.py
@@ -501,9 +501,9 @@
     @pl.loop(0, 2 * far + 1)
     def _(v):
         u = v - far
-        pl.when(jnp.logical_or(v < far, u == far))(lambda: take_before(jnp.minimum(v, far)))
-
-        @pl.when(v == 1)
+        pl.when(v <= far)(lambda: take_before(v))
+
+        @pl.when(v == far - 1)
         def _():
             @pl.loop(1, far)
             def _(k):

time: 124 us -> 124 us (level)
  no operation moved by 1% of the time
where the time goes in v7:
time: 124 us
  Pallas kernels  122 us (98%)
  local copies, waits for them, and re-layouts  1.87 us (2%)
    pallas_call x1, Pallas kernels, on_device(): pl.pallas_call(functools.partial(layer_kernel, L, G, cap, tile), out_shap...  122 us

profile of v7, /device:TPU:0, one launch (start us, length us, event | category | flops | bytes accessed | tf_op | source)
XLA Modules:
  0.0 123.8 jit_solution(13642709045669652647)
XLA Ops:
  0.0 121.9 %layer.1 = bf16[1024,256]{1,0:T(8,128)(2,1)} custom-call(bf16[1024,256]{1,0:T(8,128)(2,1)} %x_ref.1, bf16[256]{0:T(256)(128)(2,1)} %pre_ref.1, bf16[256]{0:T(256)(128)(2,1)} %post_ref.1, s32[2,1024]{1,0:T(2,128)} %bitcast.8, f32[2,1024]{1,0:T(2,128)} %bitcast.9, bf16[2048,896]{1,0:T(8,128)(2,1)} %bitcast.5, bf16[2048,896]{1,0:T(8,128)(2,1)} %bitcast.6, ...), custom_call_target="tpu_custom_call" | custom-call | tf_op jit(solution)/shard_map/layer/pallas_call | solution.py:699
  121.9 1.9 %copy.10 = bf16[1024,256]{1,0:T(8,128)(2,1)} copy(bf16[1024,256]{1,0:T(8,128)(2,1)} %layer.1) | data formatting | bytes 1048576
